TPU v7x, 1024 devices: a 2x16x16 block of a 4x16x16 slice. The times are simulated.
1024 devices in a mesh: grp: 2 (over x), tp: 16 (over z), dp: 32 (over y, core).
Axes of the slice: x: 2, y: 16, z: 16, core: 2. Of those that a mesh axis runs over, the one named last changes fastest.
The devices are a block of a 4x16x16 slice.
Arguments:
- hidden: bfloat16 [128, 2048], P('grp', 'dp'), parts along dimension 0, may hold values from -20 to 20
- lengths: int32 [128], P(('grp', 'dp')), parts along dimension 0, may hold values from 1 to 256, 4096 in all
- input_norm_gain: float32 [2, 2048], P(None, 'dp'), may hold values from 0.1 to 1.9
- gate_matrix: bfloat16 [2, 2048, 4096], P(None, 'dp', 'tp'), may hold values from -0.125 to 0.125
- input_matrix: bfloat16 [2, 2048, 4096], P(None, 'dp', 'tp'), may hold values from -0.125 to 0.125
- write_matrix: bfloat16 [2, 2048, 2048], P(None, 'dp', 'tp'), may hold values from -0.125 to 0.125
- read_matrix: bfloat16 [2, 2048, 2048], P(None, 'dp', 'tp'), may hold values from -0.125 to 0.125
- step_matrix: bfloat16 [2, 2048, 64], P(None, 'dp'), may hold values from -0.125 to 0.125
- step_size_bias: float32 [2, 64], P(None, 'tp'), may hold values from -2 to 1
- log_decay_rate: float32 [2, 64], P(None, 'tp'), may hold values from -1 to 2
- direct_path_gain: float32 [2, 64], P(None, 'tp'), may hold values from 0.5 to 1.5
- input_filter_taps: bfloat16 [2, 4, 4096], P(None, None, 'tp'), may hold values from -3 to 3
- write_filter_taps: bfloat16 [2, 4, 2048], P(None, None, 'tp'), may hold values from -3 to 3
- read_filter_taps: bfloat16 [2, 4, 2048], P(None, None, 'tp'), may hold values from -3 to 3
- position_log_decay: float32 [2, 256, 64], P(None, None, 'tp'), may hold values from -0.7 to 0
- grouped_norm_gain: float32 [2, 4096], P(None, 'tp'), may hold values from 0.1 to 1.9
- output_matrix: bfloat16 [2, 4096, 2048], P(None, 'tp', 'dp'), may hold values from -0.09375 to 0.09375
- recurrent_head_state: float32 [2, 128, 64, 64, 128], P(None, ('grp', 'dp'), 'tp'), parts along dimension 1, may hold values from -3 to 3
- history_input_rows: bfloat16 [2, 128, 3, 4096], P(None, ('grp', 'dp'), None, 'tp'), parts along dimension 1, may hold values from -5 to 5
- history_write_rows: bfloat16 [2, 128, 3, 2048], P(None, ('grp', 'dp'), None, 'tp'), parts along dimension 1, may hold values from -5 to 5
- history_read_rows: bfloat16 [2, 128, 3, 2048], P(None, ('grp', 'dp'), None, 'tp'), parts along dimension 1, may hold values from -5 to 5
Outputs:
- stream_out: bfloat16 [128, 2048], P('grp', 'dp'), parts along dimension 0
- state_out: float32 [2, 128, 64, 64, 128], P(None, ('grp', 'dp'), 'tp'), parts along dimension 1
- buffer_value_out: bfloat16 [2, 128, 3, 4096], P(None, ('grp', 'dp'), None, 'tp'), parts along dimension 1
- buffer_write_out: bfloat16 [2, 128, 3, 2048], P(None, ('grp', 'dp'), None, 'tp'), parts along dimension 1
- buffer_read_out: bfloat16 [2, 128, 3, 2048], P(None, ('grp', 'dp'), None, 'tp'), parts along dimension 1
There are 2 independent parts, one for each index of `grp`. A program takes and returns all parts, laid end to end along the dimension named above; an argument that names none is the same for every part. Nothing has to cross between parts.
Inputs may be any that keep to these rules, and one draw needn't show every extreme that they name: `lengths`: a sequence's current token stands at position length - 1; some sequence has length 256.
All inputs are finite; a program needn't handle non-finite values. No bound on the sum of `lengths` on one device may be relied on, other than what follows from the above.
Results may differ from a plain program's by a relative error of at most 0.0065.
Values may be sent and summed in bfloat16 or wider, within the bound.
A program may use at most 32 MiB of HBM per device.

v0:
```python
import jax
import jax.numpy as jnp
from jax import lax
from jax.sharding import PartitionSpec as P

D = 2048


epsilon = 1e-06


def cut_along(array, dim, peers):
    dims = array.shape
    pieces = array.reshape(*dims[:dim], peers, dims[dim] // peers, *dims[dim + 1 :])
    return jnp.moveaxis(pieces, dim, 0)


def sent_and_summed(array, axis, dim):
    pieces = cut_along(array, dim, lax.axis_size(axis))
    arrived = lax.all_to_all(pieces, axis, split_axis=0, concat_axis=0, tiled=True)
    return arrived.sum(axis=0)


def in_one_piece(arrays, axis, dim, along):
    both = jnp.concatenate(arrays, axis=along)
    result, at, gathered = (sent_and_summed(both, axis, dim), 0, [])
    for a in arrays:
        gathered.append(lax.slice_in_dim(result, at, at + a.shape[along], axis=along))
        at += a.shape[along]
    return tuple(gathered)


def laid_out(pieces, dim):
    pieces = jnp.moveaxis(pieces, 0, dim)
    dims = pieces.shape
    return pieces.reshape(*dims[:dim], dims[dim] * dims[dim + 1], *dims[dim + 2 :])


def sent_to_all(array, axis):
    copies = jnp.broadcast_to(array, (lax.axis_size(axis), *array.shape))
    return lax.all_to_all(copies, axis, split_axis=0, concat_axis=0, tiled=True)


def collect(array, axis, dim):
    return laid_out(sent_to_all(array, axis), dim)


def convolve(buffer, new_row, weights, tap_valid):
    tap_rows = weights.astype(jnp.float32)
    depth = weights.shape[0] - 1
    summed = new_row.astype(jnp.float32) * tap_rows[depth]
    for k in range(depth):
        summed = summed + buffer[:, k].astype(jnp.float32) * tap_rows[k] * tap_valid[:, k : k + 1]
    shifted = jnp.concatenate([buffer[:, 1:], new_row[:, None]], axis=1)
    return (jax.nn.silu(summed), shifted)


def spread_groups(rows, seq_local, groups_local, per_group, state_dim):
    grouped = rows.reshape(seq_local, groups_local, 1, state_dim)
    return jnp.broadcast_to(grouped, (seq_local, groups_local, per_group, state_dim)).reshape(
        seq_local, groups_local * per_group, state_dim
    )


def on_device(
    hidden,
    lengths,
    input_norm_gain,
    gate_matrix,
    input_matrix,
    write_matrix,
    read_matrix,
    step_matrix,
    step_size_bias,
    log_decay_rate,
    direct_path_gain,
    input_filter_taps,
    write_filter_taps,
    read_filter_taps,
    position_log_decay,
    grouped_norm_gain,
    output_matrix,
    recurrent_head_state,
    history_input_rows,
    history_write_rows,
    history_read_rows,
):
    seq_local = lengths.shape[0]
    heads_local = step_size_bias.shape[1]
    head_dim = recurrent_head_state.shape[3]
    state_dim = recurrent_head_state.shape[4]
    groups_local = write_filter_taps.shape[2] // state_dim
    per_group = heads_local // groups_local
    inner_local = heads_local * head_dim
    shared_local = groups_local * state_dim
    depth = input_filter_taps.shape[1] - 1
    token_position = lengths - 1
    tap_valid = (jnp.arange(depth)[None, :] >= depth - token_position[:, None]).astype(jnp.float32)
    state_is_valid = (token_position > 0).astype(jnp.float32)[:, None]
    position_indicator = (
        token_position[:, None] == jnp.arange(position_log_decay.shape[1])[None, :]
    ).astype(jnp.float32)
    head_first = lax.axis_index("tp") * heads_local
    share_rows = hidden.shape[0] // lax.axis_size("tp")
    share_first = lax.axis_index("tp") * share_rows
    stream = hidden
    states, values, writes, reads = ([], [], [], [])
    for layer_index in range(input_norm_gain.shape[0]):
        stream_float = stream.astype(jnp.float32)
        squares = jnp.sum(stream_float * stream_float, axis=1)
        normed = (stream_float * input_norm_gain[layer_index]).astype(jnp.bfloat16)
        pieces = [
            jnp.dot(normed, weight[layer_index], preferred_element_type=jnp.float32)
            for weight in (gate_matrix, input_matrix, write_matrix, read_matrix)
        ]
        joined = jnp.concatenate(pieces, axis=1)
        step_weight = step_matrix[layer_index]
        step_term = jnp.dot(normed, step_weight, preferred_element_type=jnp.float32)
        joined_mine, step_mine, squares_mine = in_one_piece(
            (joined, step_term, squares[:, None]), "dp", 0, 1
        )
        mean_square = squares_mine[:, 0] / D
        row_scale = lax.rsqrt(mean_square + epsilon)[:, None]
        step_raw = lax.dynamic_slice_in_dim(step_mine, head_first, heads_local, 1) * row_scale
        scaled = joined_mine * row_scale
        proj_gate = scaled[:, :inner_local]
        value_row = scaled[:, inner_local : 2 * inner_local].astype(jnp.bfloat16)
        write_row = scaled[:, 2 * inner_local : 2 * inner_local + shared_local].astype(jnp.bfloat16)
        read_row = scaled[:, 2 * inner_local + shared_local :].astype(jnp.bfloat16)
        value_act, value_buf = convolve(
            history_input_rows[layer_index], value_row, input_filter_taps[layer_index], tap_valid
        )
        write_act, write_buf = convolve(
            history_write_rows[layer_index], write_row, write_filter_taps[layer_index], tap_valid
        )
        read_act, read_buf = convolve(
            history_read_rows[layer_index], read_row, read_filter_taps[layer_index], tap_valid
        )
        head_step_size = jax.nn.softplus(step_raw + step_size_bias[layer_index])
        current_log_decay = jnp.dot(
            position_indicator, position_log_decay[layer_index], precision=lax.Precision.HIGHEST
        )
        current_decay = (
            jnp.exp(-jnp.exp(log_decay_rate[layer_index]) * head_step_size + current_log_decay)
            * state_is_valid
        )
        value_heads = value_act.reshape(seq_local, heads_local, head_dim)
        write_heads = spread_groups(write_act, seq_local, groups_local, per_group, state_dim)
        read_heads = spread_groups(read_act, seq_local, groups_local, per_group, state_dim)
        updated = (
            current_decay[:, :, None, None] * recurrent_head_state[layer_index]
            + (head_step_size[:, :, None] * value_heads)[:, :, :, None] * write_heads[:, :, None, :]
        )
        readout = jnp.einsum("shpn,shn->shp", updated, read_heads, precision=lax.Precision.HIGHEST)
        mixed_heads = (
            readout + direct_path_gain[layer_index][None, :, None] * value_heads
        ) * jax.nn.silu(proj_gate.reshape(seq_local, heads_local, head_dim))
        grouped = mixed_heads.reshape(seq_local, groups_local, per_group * head_dim)
        grouped = grouped * lax.rsqrt(jnp.mean(grouped * grouped, axis=2, keepdims=True) + epsilon)
        gated_rows = (
            grouped.reshape(seq_local, inner_local) * grouped_norm_gain[layer_index]
        ).astype(jnp.bfloat16)
        out_weight = output_matrix[layer_index]

        def project(rows_in, first_row, out_weight=out_weight):
            return jnp.dot(rows_in, out_weight, preferred_element_type=jnp.float32)

        partial_out = project(collect(gated_rows, "dp", 0), jnp.int32(0))
        branch_share = sent_and_summed(partial_out, "tp", 0)
        stream_share = lax.dynamic_slice_in_dim(stream_float, share_first, share_rows, 0)
        new_share = (stream_share + branch_share).astype(jnp.bfloat16)
        stream = collect(new_share, "tp", 0)
        states.append(updated)
        values.append(value_buf)
        writes.append(write_buf)
        reads.append(read_buf)
    return (stream, jnp.stack(states), jnp.stack(values), jnp.stack(writes), jnp.stack(reads))


def solution(mesh):
    placed = (
        P("grp", "dp"),
        P(("grp", "dp")),
        P(None, "dp"),
        P(None, "dp", "tp"),
        P(None, "dp", "tp"),
        P(None, "dp", "tp"),
        P(None, "dp", "tp"),
        P(None, "dp", None),
        P(None, "tp"),
        P(None, "tp"),
        P(None, "tp"),
        P(None, None, "tp"),
        P(None, None, "tp"),
        P(None, None, "tp"),
        P(None, None, "tp"),
        P(None, "tp"),
        P(None, "tp", "dp"),
        P(None, ("grp", "dp"), "tp", None, None),
        P(None, ("grp", "dp"), None, "tp"),
        P(None, ("grp", "dp"), None, "tp"),
        P(None, ("grp", "dp"), None, "tp"),
    )
    return jax.shard_map(
        on_device,
        mesh=mesh,
        in_specs=placed,
        out_specs=(
            P("grp", "dp"),
            P(None, ("grp", "dp"), "tp", None, None),
            P(None, ("grp", "dp"), None, "tp"),
            P(None, ("grp", "dp"), None, "tp"),
            P(None, ("grp", "dp"), None, "tp"),
        ),
        check_vma=False,
    )
```

profile of v0, /device:TPU:6, one launch (start us, length us, event | category | flops | bytes accessed | tf_op | source)
XLA Modules:
  0.0 256.6 jit_solution(5951249357606938407)
XLA Ops:
  0.6 0.8 slice_bitcast_fusion.36
  1.4 0.8 multiply_reduce_fusion.1
  2.2 0.1 concatenate.30
  2.3 0.3 copy.52
  2.6 0.3 copy-done.5
  3.0 0.1 fusion.50
  3.1 0.6 copy-done.6
  3.7 0.1 fusion.48
  3.9 0.1 fusion.46
  4.0 0.6 copy-done.1
  4.6 0.1 fusion.28
  4.7 0.7 copy-done.2
  5.4 0.1 fusion.30
  5.7 0.9 copy.53
  6.6 15.3 %all-to-all-start = ((f32[32,2,833]{2,1,0:T(2,128)}), f32[32,2,833]{2,1,0:T(2,128)S(1)}, u32[]{:S(2)}, u32[]{:S(2)}) async-start(f32[32,2,833]{2,1,0:T(2,128)} %copy.53), calls=%async_computation | async-start | bytes 458752 | tf_op jit(solution)/shard_map/all_to_all | solution.py:20
  22.2 0.6 copy-done.10
  22.8 0.7 copy-done.9
  23.5 19.1 %all-to-all-done = f32[32,2,833]{2,1,0:T(2,128)S(1)} async-done(((f32[32,2,833]{2,1,0:T(2,128)}), f32[32,2,833]{2,1,0:T(2,128)S(1)}, u32[]{:S(2)}, u32[]{:S(2)}) %all-to-all-start) | async-done | bytes 213280 | tf_op jit(solution)/shard_map/all_to_all | solution.py:20
  42.7 0.2 fusion.117
  43.4 0.5 copy-done.18
  43.9 0.2 fusion.2
  44.2 0.6 fusion.8
  44.8 0.2 multiply_reduce_fusion.3
  45.2 16.1 %all_to_all.40 = bf16[32,2,256]{2,1,0:T(2,128)(2,1)S(1)} all-to-all(bf16[32,2,256]{2,1,0:T(2,128)(2,1)S(1)} %broadcast_in_dim.20), channel_id=1, replica_groups=mesh['grp'=2,'tp'=16,'dp'=32] {'dp'}, dimensions={0} | all-to-all | bytes 65536 | tf_op jit(solution)/shard_map/all_to_all | solution.py:41
  61.4 0.1 fusion.26
  61.6 0.7 reshape.343
  62.3 83.2 %all-to-all-start.2 = ((f32[16,1,256]{2,1,0:T(1,128)}), f32[16,1,256]{2,1,0:T(1,128)S(1)}, u32[]{:S(2)}, u32[]{:S(2)}) async-start(f32[16,1,256]{2,1,0:T(1,128)} %reshape.343), calls=%async_computation.2 | async-start | bytes 32768 | tf_op jit(solution)/shard_map/all_to_all | solution.py:20
  145.5 12.3 %all-to-all-done.2 = f32[16,1,256]{2,1,0:T(1,128)S(1)} async-done(((f32[16,1,256]{2,1,0:T(1,128)}), f32[16,1,256]{2,1,0:T(1,128)S(1)}, u32[]{:S(2)}, u32[]{:S(2)}) %all-to-all-start.2) | async-done | bytes 16416 | tf_op jit(solution)/shard_map/all_to_all | solution.py:20
  157.8 0.5 broadcast.182
  158.3 0.7 reduce.7
  159.3 15.0 %all_to_all.41 = bf16[16,2,128]{2,1,0:T(2,128)(2,1)S(1)} all-to-all(bf16[16,2,128]{2,1,0:T(2,128)(2,1)S(1)} %reshape.345), channel_id=1, replica_groups=mesh['grp'=2,'tp'=16,'dp'=32] {'tp'}, dimensions={0} | all-to-all | bytes 16384 | tf_op jit(solution)/shard_map/all_to_all | solution.py:41
  174.4 0.1 multiply_reduce_fusion
  174.5 0.1 fusion.44
  174.6 0.1 fusion.42
  174.7 0.1 fusion.40
  174.9 0.1 fusion.22
  175.0 0.1 fusion.24
  175.2 0.3 copy.61
  175.5 0.1 concatenate.33
  175.6 0.9 copy.62
  176.5 4.8 %all-to-all-start.4 = ((f32[32,2,833]{2,1,0:T(2,128)}), f32[32,2,833]{2,1,0:T(2,128)S(1)}, u32[]{:S(2)}, u32[]{:S(2)}) async-start(f32[32,2,833]{2,1,0:T(2,128)} %copy.62), calls=%async_computation.4 | async-start | bytes 458752 | tf_op jit(solution)/shard_map/all_to_all | solution.py:20
  181.4 20.4 %all-to-all-done.4 = f32[32,2,833]{2,1,0:T(2,128)S(1)} async-done(((f32[32,2,833]{2,1,0:T(2,128)}), f32[32,2,833]{2,1,0:T(2,128)S(1)}, u32[]{:S(2)}, u32[]{:S(2)}) %all-to-all-start.4) | async-done | bytes 213280 | tf_op jit(solution)/shard_map/all_to_all | solution.py:20
  201.9 0.2 fusion.118
  202.5 0.2 fusion.3
  202.8 0.1 divide_multiply_fusion.5
  202.9 0.2 multiply_add_fusion.1
  203.2 0.6 fusion.5
  203.8 0.2 multiply_reduce_fusion.2
  204.1 0.6 broadcast_in_dim.22
  204.8 4.7 %all-to-all-start.5 = ((bf16[32,2,256]{2,1,0:T(2,128)(2,1)}), bf16[32,2,256]{2,1,0:T(2,128)(2,1)S(1)}, u32[]{:S(2)}, u32[]{:S(2)}) async-start(bf16[32,2,256]{2,1,0:T(2,128)(2,1)} %broadcast_in_dim.22), calls=%async_computation.5 | async-start | bytes 65536 | tf_op jit(solution)/shard_map/all_to_all | solution.py:41
  209.5 0.6 pad_maximum_fusion.1
  210.1 0.6 pad_maximum_fusion.3
  210.7 0.8 pad_maximum_fusion
  211.5 10.1 %all-to-all-done.5 = bf16[32,2,256]{2,1,0:T(2,128)(2,1)S(1)} async-done(((bf16[32,2,256]{2,1,0:T(2,128)(2,1)}), bf16[32,2,256]{2,1,0:T(2,128)(2,1)S(1)}, u32[]{:S(2)}, u32[]{:S(2)}) %all-to-all-start.5) | async-done | bytes 32800 | tf_op jit(solution)/shard_map/all_to_all | solution.py:41
  221.7 0.1 fusion.20
  221.9 0.7 reshape.347
  222.6 3.9 %all-to-all-start.6 = ((f32[16,1,256]{2,1,0:T(1,128)}), f32[16,1,256]{2,1,0:T(1,128)S(1)}, u32[]{:S(2)}, u32[]{:S(2)}) async-start(f32[16,1,256]{2,1,0:T(1,128)} %reshape.347), calls=%async_computation.6 | async-start | bytes 32768 | tf_op jit(solution)/shard_map/all_to_all | solution.py:20
  226.5 12.1 %all-to-all-done.6 = f32[16,1,256]{2,1,0:T(1,128)S(1)} async-done(((f32[16,1,256]{2,1,0:T(1,128)}), f32[16,1,256]{2,1,0:T(1,128)S(1)}, u32[]{:S(2)}, u32[]{:S(2)}) %all-to-all-start.6) | async-done | bytes 16416 | tf_op jit(solution)/shard_map/all_to_all | solution.py:20
  238.6 0.7 reduce.8
  239.4 0.7 reshape.349
  240.1 3.9 %all-to-all-start.7 = ((bf16[16,2,128]{2,1,0:T(2,128)(2,1)}), bf16[16,2,128]{2,1,0:T(2,128)(2,1)S(1)}, u32[]{:S(2)}, u32[]{:S(2)}) async-start(bf16[16,2,128]{2,1,0:T(2,128)(2,1)} %reshape.349), calls=%async_computation.7 | async-start | bytes 16384 | tf_op jit(solution)/shard_map/all_to_all | solution.py:41
  244.0 0.6 pad_maximum_fusion.2
  244.6 11.3 %all-to-all-done.7 = bf16[16,2,128]{2,1,0:T(2,128)(2,1)S(1)} async-done(((bf16[16,2,128]{2,1,0:T(2,128)(2,1)}), bf16[16,2,128]{2,1,0:T(2,128)(2,1)S(1)}, u32[]{:S(2)}, u32[]{:S(2)}) %all-to-all-start.7) | async-done | bytes 8224 | tf_op jit(solution)/shard_map/all_to_all | solution.py:41
  256.0 0.7 reshape.350
  (111 shorter events, 2.6 us)
Async XLA Ops:
  2.2 0.8 copy-start.5
  3.0 0.8 copy-start.6
  3.0 0.9 copy-start.7
  3.7 0.8 copy-start.1
  4.6 0.8 copy-start.2
  5.6 16.3 %copy-start.15 = (f32[2,4]{1,0:T(2,128)S(1)}, f32[2,4]{1,0:T(2,128)}, u32[]{:S(2)}) copy-start(f32[2,4]{1,0:T(2,128)} %param.29) | copy-start | bytes 100
  5.6 16.3 %copy-start.16 = (f32[2,4]{1,0:T(2,128)S(1)}, f32[2,4]{1,0:T(2,128)}, u32[]{:S(2)}) copy-start(f32[2,4]{1,0:T(2,128)} %param.30) | copy-start | bytes 100
  5.7 16.3 %copy-start.17 = (f32[2,4]{1,0:T(2,128)S(1)}, f32[2,4]{1,0:T(2,128)}, u32[]{:S(2)}) copy-start(f32[2,4]{1,0:T(2,128)} %param.31) | copy-start | bytes 100
  5.7 16.3 %copy-start.19 = (s32[2]{0:T(128)S(1)}, s32[2]{0:T(128)}, u32[]{:S(2)}) copy-start(s32[2]{0:T(128)} %param.22) | copy-start | bytes 28
  5.7 16.3 %copy-start.14 = (f32[2,256]{1,0:T(2,128)S(1)}, f32[2,256]{1,0:T(2,128)}, u32[]{:S(2)}) copy-start(f32[2,256]{1,0:T(2,128)} %param.36) | copy-start | bytes 6148
  5.7 16.4 %copy-start.12 = (bf16[2,4,128]{2,1,0:T(4,128)(2,1)S(1)}, bf16[2,4,128]{2,1,0:T(4,128)(2,1)}, u32[]{:S(2)}) copy-start(bf16[2,4,128]{2,1,0:T(4,128)(2,1)} %param.33) | copy-start | bytes 6148
  5.7 16.4 %copy-start.13 = (bf16[2,4,128]{2,1,0:T(4,128)(2,1)S(1)}, bf16[2,4,128]{2,1,0:T(4,128)(2,1)}, u32[]{:S(2)}) copy-start(bf16[2,4,128]{2,1,0:T(4,128)(2,1)} %param.34) | copy-start | bytes 6148
  5.7 16.4 %copy-start.8 = (bf16[2,2,3,256]{3,1,2,0:T(2,128)(2,1)S(1)}, bf16[2,2,3,256]{3,1,2,0:T(2,128)(2,1)}, u32[]{:S(2)}) copy-start(bf16[2,2,3,256]{3,1,2,0:T(2,128)(2,1)} %param.39) | copy-start | bytes 18436
  6.6 37.6 %copy-start = (f32[2,2,4,64,128]{4,3,2,1,0:T(8,128)S(1)}, f32[2,2,4,64,128]{4,3,2,1,0:T(8,128)}, u32[]{:S(2)}) copy-start(f32[2,2,4,64,128]{4,3,2,1,0:T(8,128)} %param.38) | copy-start | bytes 1572868
  6.6 36.0 %all-to-all-start = ((f32[32,2,833]{2,1,0:T(2,128)}), f32[32,2,833]{2,1,0:T(2,128)S(1)}, u32[]{:S(2)}, u32[]{:S(2)}) async-start(f32[32,2,833]{2,1,0:T(2,128)} %copy.53), calls=%async_computation | async-start | bytes 458752 | tf_op jit(solution)/shard_map/all_to_all | solution.py:20
  22.1 0.7 copy-start.10
  22.1 0.7 copy-start.11
  22.8 0.7 copy-start.9
  43.2 0.7 copy-start.18
  45.2 16.2 %copy-start.3 = (bf16[2,256,64]{1,2,0:T(8,128)(2,1)S(1)}, bf16[2,256,64]{1,2,0:T(8,128)(2,1)}, u32[]{:S(2)}) copy-start(bf16[2,256,64]{1,2,0:T(8,128)(2,1)} %param.37) | copy-start | bytes 196612
  62.3 83.2 %copy-start.4 = (bf16[64,64]{1,0:T(8,128)(2,1)S(1)}, bf16[64,64]{1,0:T(8,128)(2,1)}, u32[]{:S(2)}) copy-start(bf16[64,64]{1,0:T(8,128)(2,1)} %param.21) | copy-start | bytes 24580
  62.3 95.5 %all-to-all-start.2 = ((f32[16,1,256]{2,1,0:T(1,128)}), f32[16,1,256]{2,1,0:T(1,128)S(1)}, u32[]{:S(2)}, u32[]{:S(2)}) async-start(f32[16,1,256]{2,1,0:T(1,128)} %reshape.343), calls=%async_computation.2 | async-start | bytes 32768 | tf_op jit(solution)/shard_map/all_to_all | solution.py:20
  176.5 25.4 %all-to-all-start.4 = ((f32[32,2,833]{2,1,0:T(2,128)}), f32[32,2,833]{2,1,0:T(2,128)S(1)}, u32[]{:S(2)}, u32[]{:S(2)}) async-start(f32[32,2,833]{2,1,0:T(2,128)} %copy.62), calls=%async_computation.4 | async-start | bytes 458752 | tf_op jit(solution)/shard_map/all_to_all | solution.py:20
  204.8 16.9 %all-to-all-start.5 = ((bf16[32,2,256]{2,1,0:T(2,128)(2,1)}), bf16[32,2,256]{2,1,0:T(2,128)(2,1)S(1)}, u32[]{:S(2)}, u32[]{:S(2)}) async-start(bf16[32,2,256]{2,1,0:T(2,128)(2,1)} %broadcast_in_dim.22), calls=%async_computation.5 | async-start | bytes 65536 | tf_op jit(solution)/shard_map/all_to_all | solution.py:41
  222.6 16.0 %all-to-all-start.6 = ((f32[16,1,256]{2,1,0:T(1,128)}), f32[16,1,256]{2,1,0:T(1,128)S(1)}, u32[]{:S(2)}, u32[]{:S(2)}) async-start(f32[16,1,256]{2,1,0:T(1,128)} %reshape.347), calls=%async_computation.6 | async-start | bytes 32768 | tf_op jit(solution)/shard_map/all_to_all | solution.py:20
  240.1 15.9 %all-to-all-start.7 = ((bf16[16,2,128]{2,1,0:T(2,128)(2,1)}), bf16[16,2,128]{2,1,0:T(2,128)(2,1)S(1)}, u32[]{:S(2)}, u32[]{:S(2)}) async-start(bf16[16,2,128]{2,1,0:T(2,128)(2,1)} %reshape.349), calls=%async_computation.7 | async-start | bytes 16384 | tf_op jit(solution)/shard_map/all_to_all | solution.py:41
where the time goes:
time: 258 us; the launch traced here: 257 us
  starting transfers between devices  116 us (45%)
  waiting for transfers between devices  85.3 us (33%)
  blocking collectives  31.2 us (12%)
  local copies, waits for them, and re-layouts  12.7 us (5%)
  other arithmetic  7.19 us (3%)
  matrix products  3.07 us (1%)
    all_to_all x4, starting transfers between devices, sent_and_summed(): lax.all_to_all(pieces, axis, split_axis=0, concat_axis=0, tiled=True)  107 us
    all_to_all x4, waiting for transfers between devices, sent_and_summed(): lax.all_to_all(pieces, axis, split_axis=0, concat_axis=0, tiled=True)  63.9 us
    all_to_all x2, blocking collectives, sent_to_all(): return lax.all_to_all(copies, axis, split_axis=0, concat_axis=0, tiled=True)  31.2 us
    all_to_all x2, waiting for transfers between devices, sent_to_all(): return lax.all_to_all(copies, axis, split_axis=0, concat_axis=0, tiled=True)  21.5 us
    all_to_all x2, starting transfers between devices, sent_to_all(): return lax.all_to_all(copies, axis, split_axis=0, concat_axis=0, tiled=True)  8.64 us
    unnamed x48, local copies, waits for them, and re-layouts  7.33 us
  transfers between devices with their start and end apart: 6, of which 6 were waited for; matrix products, arithmetic and copies ran while one was open for 1% of the time, Pallas kernels for 0%

commit v1 on v0

v1 whole, which is shorter than its diff:
```python
import functools

import jax
import jax.numpy as jnp
from jax import lax
from jax.experimental import pallas as pl
from jax.experimental.pallas import tpu as pltpu
from jax.sharding import PartitionSpec as P

MESH = pl.DeviceIdType.MESH
F32 = jnp.float32
BF16 = jnp.bfloat16
epsilon = 1e-06
LANES = 128
BLOCKS = 8
HIGH = lax.Precision.HIGHEST
LAST = (((1,), (1,)), ((), ()))


def far_first(count):
    return sorted(range(1, count), key=lambda o: -min(o, count - o))


def silu(z):
    return z / (1.0 + jnp.exp(-z))


def high_part(v):
    return v.astype(BF16).astype(F32)


def wait_bytes(ref, sem):
    pltpu.make_async_copy(ref, ref, sem).wait()


def lane_rows(block, first):
    return jnp.concatenate([block[first : first + 1], block[first + 1 : first + 2]], axis=1)


def kernel(
    n_dp,
    n_tp,
    hidden,
    lengths,
    in_gain,
    w_gate,
    w_value,
    w_write,
    w_read,
    w_step,
    step_bias,
    log_rate,
    direct_gain,
    taps_value,
    taps_write,
    taps_read,
    log_decay,
    group_gain,
    w_out,
    state_in,
    hist_value,
    hist_write,
    hist_read,
    stream_out,
    state_out,
    buf_value,
    buf_write,
    buf_read,
    part,
    rs_send,
    rs_recv,
    ag_send,
    ag_recv,
    gathered,
    ar_send,
    ar_recv,
    state,
    state_new,
    state_hi,
    state_lo,
    w_pack,
    conv_base,
    conv_last,
    tap_rows,
    decay_pad,
    head_pad,
    rs_ssem,
    rs_rsem,
    ag_ssem,
    ag_rsem,
    ar_ssem,
    ar_rsem,
    state_isem,
    state_osem,
):
    dp, tp = lax.axis_index("dp"), lax.axis_index("tp")
    layers, feats = in_gain.shape
    seqs = hidden.shape[0]
    width = feats * n_dp
    heads = step_bias.shape[1]
    inner = w_gate.shape[2]
    head_dim = inner // heads
    depth = hist_value.shape[1]
    half = seqs // 2

    barrier = pltpu.get_barrier_semaphore()
    for o in far_first(n_dp):
        pl.semaphore_signal(barrier, inc=1, device_id={"dp": lax.rem(dp + o, n_dp)}, device_id_type=MESH)
    for o in far_first(n_tp):
        pl.semaphore_signal(barrier, inc=1, device_id={"tp": lax.rem(tp + o, n_tp)}, device_id_type=MESH)
    loads = [pltpu.make_async_copy(state_in.at[l], state.at[l], state_isem.at[l]) for l in range(layers)]
    for c in loads:
        c.start()

    lane_seq = lax.broadcasted_iota(jnp.int32, (seqs, LANES), 1)
    lane_inner = lax.broadcasted_iota(jnp.int32, (2, inner), 1)
    pick = (
        lax.broadcasted_iota(jnp.int32, (w_step.shape[2], LANES), 0)
        == lax.broadcasted_iota(jnp.int32, (w_step.shape[2], LANES), 1) + tp * heads
    ) & (lax.broadcasted_iota(jnp.int32, (w_step.shape[2], LANES), 1) < heads)
    pick = pick.astype(F32).astype(BF16)

    def per_head(rows):
        out = jnp.broadcast_to(rows[:, heads - 1 : heads], (rows.shape[0], inner))
        lane = lane_inner[: rows.shape[0]]
        for h in range(heads - 2, -1, -1):
            out = jnp.where(lane < (h + 1) * head_dim, rows[:, h : h + 1], out)
        return out

    def project(l, x):
        normed = (x * in_gain[l : l + 1, :]).astype(BF16)
        columns = []
        for w in (w_gate, w_value, w_write, w_read):
            r = jnp.dot(normed, w[l], preferred_element_type=F32)
            for at in range(0, r.shape[1], LANES):
                columns.append(r[:, at : at + LANES])
        w_mine = jnp.dot(w_step[l], pick, preferred_element_type=F32).astype(BF16)
        step = jnp.dot(normed, w_mine, preferred_element_type=F32)
        square = jnp.sum(x * x, axis=1, keepdims=True)
        rest = jnp.where(lane_seq == heads, square, step)
        high = high_part(rest)
        columns += [high, rest - high]
        for c, column in enumerate(columns):
            part[pl.ds(c, seqs, stride=BLOCKS), :] = column
        rs_send[l] = part[...].reshape(n_dp, 2 * BLOCKS, LANES).astype(BF16)

    def send_partials(l):
        for o in far_first(n_dp):
            to = lax.rem(dp + o, n_dp)
            pltpu.make_async_remote_copy(
                src_ref=rs_send.at[l, to],
                dst_ref=rs_recv.at[l, dp],
                send_sem=rs_ssem.at[l],
                recv_sem=rs_rsem.at[l],
                device_id={"dp": to},
                device_id_type=MESH,
            ).start()
        rs_recv[l, dp] = rs_send[l, dp]

    def send_gated(l):
        for o in far_first(n_dp):
            pltpu.make_async_remote_copy(
                src_ref=ag_send.at[l],
                dst_ref=ag_recv.at[l, dp],
                send_sem=ag_ssem.at[l],
                recv_sem=ag_rsem.at[l],
                device_id={"dp": lax.rem(dp + o, n_dp)},
                device_id_type=MESH,
            ).start()
        ag_recv[l, dp] = ag_send[l]

    def send_branch(l):
        for o in far_first(n_tp):
            pltpu.make_async_remote_copy(
                src_ref=ar_send.at[l],
                dst_ref=ar_recv.at[l, tp],
                send_sem=ar_ssem.at[l],
                recv_sem=ar_rsem.at[l],
                device_id={"tp": lax.rem(tp + o, n_tp)},
                device_id_type=MESH,
            ).start()
        ar_recv[l, tp] = ar_send[l]

    x_bf = hidden[...]
    project(0, x_bf.astype(F32))

    position = [lengths[s] - 1 for s in range(2)]
    row8 = lax.broadcasted_iota(jnp.int32, (8, log_decay.shape[2]), 0)
    lane_pos = lax.broadcasted_iota(jnp.int32, (8, log_decay.shape[2]), 1)
    at_position = (lane_pos == jnp.where(row8 == 0, position[0], position[1])).astype(F32)
    row2 = lax.broadcasted_iota(jnp.int32, (2, LANES), 0)
    is_live = jnp.where(jnp.where(row2 == 0, position[0], position[1]) > 0, 1.0, 0.0)
    conv_base[...] = jnp.zeros_like(conv_base)
    conv_last[...] = jnp.zeros_like(conv_last)
    decay_pad[...] = jnp.zeros_like(decay_pad)
    head_pad[...] = jnp.zeros_like(head_pad)
    w_pack[...] = jnp.zeros_like(w_pack)
    decay_log = []
    for l in range(layers):
        decay_pad[l, 0:heads, :] = log_decay[l]
        picked = lax.dot_general(at_position, decay_pad[l], LAST, precision=HIGH, preferred_element_type=F32)
        decay_log.append(picked[0:2])
        head_pad[l, 0:1, 0:heads] = step_bias[l : l + 1, :]
        head_pad[l, 1:2, 0:heads] = jnp.exp(log_rate[l : l + 1, :])
        w_pack[l, 0:feats, 0:inner] = w_out[l]
        w_pack[l, feats : 2 * feats, inner : 2 * inner] = w_out[l]
        for taps, hist, row in (
            (taps_value, hist_value, 2),
            (taps_write, hist_write, 4),
            (taps_read, hist_read, 5),
        ):
            tap = taps[l].astype(F32)
            total = None
            for k in range(depth):
                rows = hist[l, k].astype(F32)
                valid = jnp.where(
                    lax.broadcasted_iota(jnp.int32, rows.shape, 0) == 0,
                    jnp.where(k >= depth - position[0], 1.0, 0.0),
                    jnp.where(k >= depth - position[1], 1.0, 0.0),
                )
                term = rows * tap[k : k + 1] * valid
                total = term if total is None else total + term
            for c in range(rows.shape[1] // LANES):
                for s in range(2):
                    at = s * BLOCKS + row + c
                    conv_base[l, at : at + 1, :] = total[s : s + 1, c * LANES : (c + 1) * LANES]
                    conv_last[l, at : at + 1, :] = tap[depth : depth + 1, c * LANES : (c + 1) * LANES]
    for l in range(layers):
        loads[l].wait()
        high = state[l].astype(BF16)
        state_hi[l] = high
        state_lo[l] = (state[l] - high.astype(F32)).astype(BF16)

    pl.semaphore_wait(barrier, n_dp - 1 + n_tp - 1)

    row16 = lax.broadcasted_iota(jnp.int32, (2 * BLOCKS, LANES), 0)
    is_gate = lax.rem(row16, BLOCKS) < 2
    row_of8 = lax.broadcasted_iota(jnp.int32, (8, LANES), 0)
    stores = []
    x_pack = jnp.concatenate([x_bf[:half].astype(F32), x_bf[half:].astype(F32)], axis=1)
    for l in range(layers):
        send_partials(l)
        wait_bytes(rs_recv.at[l, pl.ds(0, n_dp - 1)], rs_rsem.at[l])
        summed = jnp.sum(rs_recv[l].astype(F32), axis=0)
        rest = jnp.concatenate(
            [summed[BLOCKS * s + 6 : BLOCKS * s + 7] + summed[BLOCKS * s + 7 : BLOCKS * s + 8] for s in range(2)], axis=0
        )
        row_scale = lax.rsqrt(rest[:, heads : heads + 1] / width + epsilon)
        scale16 = jnp.where(row16 < BLOCKS, row_scale[0:1], row_scale[1:2])
        scaled = summed * scale16
        current = high_part(scaled)
        act = silu(jnp.where(is_gate, scaled, conv_base[l] + current * conv_last[l]))
        z = rest * row_scale + head_pad[l, 0:1, :]
        step = jnp.maximum(z, 0.0) + jnp.log1p(jnp.exp(-jnp.abs(z)))
        decay = jnp.exp(decay_log[l] - head_pad[l, 1:2, :] * step) * is_live
        gate_row = jnp.concatenate([lane_rows(act, BLOCKS * s) for s in range(2)], axis=0)
        value_row = jnp.concatenate([lane_rows(act, BLOCKS * s + 2) for s in range(2)], axis=0)
        step_value = per_head(step) * value_row
        decay_row = per_head(decay)
        readout, along = [], []
        for s in range(2):
            write = act[BLOCKS * s + 4 : BLOCKS * s + 5]
            read = act[BLOCKS * s + 5 : BLOCKS * s + 6]
            high = high_part(read)
            lhs = jnp.where(row_of8 == 0, high, jnp.where(row_of8 == 1, read - high, 0.0)).astype(BF16)
            a = lax.dot_general(lhs, state_hi[l, s], LAST, preferred_element_type=F32)
            b = lax.dot_general(lhs, state_lo[l, s], LAST, preferred_element_type=F32)
            readout.append(a[0:1] + a[1:2] + b[0:1])
            along.append(jnp.sum(write * read, axis=1, keepdims=True))
        readout = jnp.concatenate(readout, axis=0)
        along = jnp.concatenate(along, axis=0)
        mixed = (
            decay_row * readout + step_value * along + per_head(direct_gain[l : l + 1, :]) * value_row
        ) * gate_row
        mean = jnp.sum(mixed * mixed, axis=1, keepdims=True) / inner
        gated = mixed * lax.rsqrt(mean + epsilon) * group_gain[l : l + 1, :]
        ag_send[l] = gated.astype(BF16)
        send_gated(l)

        for b in range(inner // LANES):
            cols = jnp.transpose(
                jnp.concatenate(
                    [step_value[:, b * LANES : (b + 1) * LANES], jnp.zeros((6, LANES), F32)], axis=0
                )
            )
            for s in range(2):
                write = act[BLOCKS * s + 4 : BLOCKS * s + 5]
                for j in range(LANES // head_dim):
                    h = b * (LANES // head_dim) + j
                    at = slice(h * head_dim, (h + 1) * head_dim)
                    state_new[l, s, at, :] = (
                        decay[s : s + 1, h : h + 1] * state[l, s, at, :]
                        + cols[j * head_dim : (j + 1) * head_dim, s : s + 1] * write
                    )
        stores.append(pltpu.make_async_copy(state_new.at[l], state_out.at[l], state_osem.at[l]))
        stores[-1].start()
        for k in range(depth - 1):
            buf_value[l, k] = hist_value[l, k + 1]
            buf_write[l, k] = hist_write[l, k + 1]
            buf_read[l, k] = hist_read[l, k + 1]
        buf_value[l, depth - 1] = jnp.concatenate(
            [lane_rows(current, BLOCKS * s + 2) for s in range(2)], axis=0
        ).astype(BF16)
        buf_write[l, depth - 1] = jnp.concatenate(
            [current[BLOCKS * s + 4 : BLOCKS * s + 5] for s in range(2)], axis=0
        ).astype(BF16)
        buf_read[l, depth - 1] = jnp.concatenate(
            [current[BLOCKS * s + 5 : BLOCKS * s + 6] for s in range(2)], axis=0
        ).astype(BF16)

        wait_bytes(ag_recv.at[l, pl.ds(0, n_dp - 1)], ag_rsem.at[l])
        for d in range(n_dp):
            gathered[2 * d : 2 * d + 2, :] = ag_recv[l, d].astype(F32)
        rows = jnp.concatenate([gathered[0:half, :], gathered[half:, :]], axis=1).astype(BF16)
        branch = lax.dot_general(rows, w_pack[l], LAST, preferred_element_type=F32)
        ar_send[l] = branch.astype(BF16)
        send_branch(l)
        wait_bytes(ar_recv.at[l, pl.ds(0, n_tp - 1)], ar_rsem.at[l])
        x_pack = high_part(x_pack + jnp.sum(ar_recv[l].astype(F32), axis=0))
        x = jnp.concatenate([x_pack[:, :feats], x_pack[:, feats:]], axis=0)
        if l + 1 < layers:
            project(l + 1, x)
    stream_out[...] = x.astype(BF16)
    for l in range(layers):
        wait_bytes(rs_send.at[l, pl.ds(0, n_dp - 1)], rs_ssem.at[l])
        wait_bytes(ag_recv.at[l, pl.ds(0, n_dp - 1)], ag_ssem.at[l])
        wait_bytes(ar_recv.at[l, pl.ds(0, n_tp - 1)], ar_ssem.at[l])
        stores[l].wait()


def on_device(
    hidden,
    lengths,
    input_norm_gain,
    gate_matrix,
    input_matrix,
    write_matrix,
    read_matrix,
    step_matrix,
    step_size_bias,
    log_decay_rate,
    direct_path_gain,
    input_filter_taps,
    write_filter_taps,
    read_filter_taps,
    position_log_decay,
    grouped_norm_gain,
    output_matrix,
    recurrent_head_state,
    history_input_rows,
    history_write_rows,
    history_read_rows,
):
    n_dp, n_tp = lax.axis_size("dp"), lax.axis_size("tp")
    layers, seq_local, heads, head_dim, state_dim = recurrent_head_state.shape
    inner = heads * head_dim
    seqs, feats = hidden.shape
    assert seq_local == 2 and state_dim == LANES and write_matrix.shape[2] == LANES and inner == 2 * LANES
    state_shape = (layers, seq_local, inner, state_dim)
    operands = (
        hidden,
        lengths,
        input_norm_gain,
        gate_matrix,
        input_matrix,
        write_matrix,
        read_matrix,
        step_matrix,
        step_size_bias,
        log_decay_rate,
        direct_path_gain,
        input_filter_taps,
        write_filter_taps,
        read_filter_taps,
        position_log_decay.transpose(0, 2, 1),
        grouped_norm_gain,
        output_matrix.transpose(0, 2, 1),
        recurrent_head_state.reshape(state_shape),
        history_input_rows.transpose(0, 2, 1, 3),
        history_write_rows.transpose(0, 2, 1, 3),
        history_read_rows.transpose(0, 2, 1, 3),
    )
    vmem, anywhere = pl.BlockSpec(memory_space=pltpu.VMEM), pl.BlockSpec(memory_space=pl.ANY)
    in_specs = [vmem] * len(operands)
    in_specs[1] = pl.BlockSpec(memory_space=pltpu.SMEM)
    in_specs[17] = anywhere
    taken = lambda a: jax.ShapeDtypeStruct(a.shape, a.dtype)
    positions = position_log_decay.shape[1]
    dma = pltpu.SemaphoreType.DMA
    stream, states, values, writes, reads = pl.pallas_call(
        functools.partial(kernel, n_dp, n_tp),
        out_shape=(
            taken(hidden),
            taken(operands[17]),
            taken(operands[18]),
            taken(operands[19]),
            taken(operands[20]),
        ),
        in_specs=in_specs,
        out_specs=(vmem, anywhere, vmem, vmem, vmem),
        scratch_shapes=[
            pltpu.VMEM((seqs * BLOCKS, LANES), F32),
            pltpu.VMEM((layers, n_dp, 2 * BLOCKS, LANES), BF16),
            pltpu.VMEM((layers, n_dp, 2 * BLOCKS, LANES), BF16),
            pltpu.VMEM((layers, 2, inner), BF16),
            pltpu.VMEM((layers, n_dp, 2, inner), BF16),
            pltpu.VMEM((seqs, inner), F32),
            pltpu.VMEM((layers, seqs // 2, 2 * feats), BF16),
            pltpu.VMEM((layers, n_tp, seqs // 2, 2 * feats), BF16),
            pltpu.VMEM(state_shape, F32),
            pltpu.VMEM(state_shape, F32),
            pltpu.VMEM(state_shape, BF16),
            pltpu.VMEM(state_shape, BF16),
            pltpu.VMEM((layers, 2 * feats, 2 * inner), BF16),
            pltpu.VMEM((layers, 2 * BLOCKS, LANES), F32),
            pltpu.VMEM((layers, 2 * BLOCKS, LANES), F32),
            pltpu.VMEM((8, LANES), F32),
            pltpu.VMEM((layers, LANES, positions), F32),
            pltpu.VMEM((layers, 8, LANES), F32),
        ]
        + [dma((layers,))] * 8,
        compiler_params=pltpu.CompilerParams(collective_id=0, has_side_effects=True),
        name="mixers",
    )(*operands)
    return (
        stream,
        states.reshape(recurrent_head_state.shape),
        values.transpose(0, 2, 1, 3),
        writes.transpose(0, 2, 1, 3),
        reads.transpose(0, 2, 1, 3),
    )


def solution(mesh):
    placed = (
        P("grp", "dp"),
        P(("grp", "dp")),
        P(None, "dp"),
        P(None, "dp", "tp"),
        P(None, "dp", "tp"),
        P(None, "dp", "tp"),
        P(None, "dp", "tp"),
        P(None, "dp", None),
        P(None, "tp"),
        P(None, "tp"),
        P(None, "tp"),
        P(None, None, "tp"),
        P(None, None, "tp"),
        P(None, None, "tp"),
        P(None, None, "tp"),
        P(None, "tp"),
        P(None, "tp", "dp"),
        P(None, ("grp", "dp"), "tp", None, None),
        P(None, ("grp", "dp"), None, "tp"),
        P(None, ("grp", "dp"), None, "tp"),
        P(None, ("grp", "dp"), None, "tp"),
    )
    return jax.shard_map(
        on_device,
        mesh=mesh,
        in_specs=placed,
        out_specs=(
            P("grp", "dp"),
            P(None, ("grp", "dp"), "tp", None, None),
            P(None, ("grp", "dp"), None, "tp"),
            P(None, ("grp", "dp"), None, "tp"),
            P(None, ("grp", "dp"), None, "tp"),
        ),
        check_vma=False,
    )
```

time: 258 us -> 151 us (0.59)
  Pallas kernels: 0 us -> 145 us
  starting transfers between devices: 116 us -> 0 us
  waiting for transfers between devices: 85.3 us -> 0 us
  blocking collectives: 31.2 us -> 0 us
  local copies, waits for them, and re-layouts: 12.7 us -> 5.13 us
  other arithmetic: 7.19 us -> 0 us
  matrix products: 3.07 us -> 0 us
    pallas_call x0 -> x1, Pallas kernels: none -> 145 us  [on_device(): pl.pallas_call(functools.partial(kernel, n_dp, n_tp), out_shape=(taken(hi...]
    all_to_all x6 -> x0, starting transfers between devices: 116 us -> none  [the longest x4 107 us: sent_and_summed(): lax.all_to_all(pieces, axis, split_axis=0, concat_axis=0, tiled=True)]
    all_to_all x6 -> x0, waiting for transfers between devices: 85.3 us -> none  [the longest x4 63.9 us: sent_and_summed(): lax.all_to_all(pieces, axis, split_axis=0, concat_axis=0, tiled=True)]
    all_to_all x2 -> x0, blocking collectives: 31.2 us -> none  [sent_to_all(): return lax.all_to_all(copies, axis, split_axis=0, concat_axis=0, tiled=True)]
    dot_general x16 -> x0, matrix products: 3.07 us -> none  [the longest x2 1.19 us: on_device(): jnp.einsum('shpn,shn->shp', updated, read_heads, precision=lax.Precision....]
    another operation x12 -> x0, other arithmetic: 2.81 us -> none  [the longest x1 0.83 us: on_device(): jnp.stack(states)]
    concatenate x8 -> x0, local copies, waits for them, and re-layouts: 2.72 us -> none  [in_one_piece(): both = jnp.concatenate(arrays, axis=along)]
    unnamed x48 -> x13, local copies, waits for them, and re-layouts: 7.33 us -> 5.13 us
  transfers between devices with their start and end apart: 6 -> 0, of which waited for: 6 -> 0; matrix products, arithmetic and copies ran while one was open for 1% -> 0% of each run, Pallas kernels for 0% -> 0%
where the time goes in v1:
time: 151 us
  Pallas kernels  145 us (96%)
  local copies, waits for them, and re-layouts  5.13 us (3%)
    pallas_call x1, Pallas kernels, on_device(): pl.pallas_call(functools.partial(kernel, n_dp, n_tp), out_shape=(taken(hi...  145 us
    unnamed x13, local copies, waits for them, and re-layouts  5.13 us

profile of v1, /device:TPU:6, one launch (start us, length us, event | category | flops | bytes accessed | tf_op | source)
XLA Modules:
  0.0 151.0 jit_solution(15786922807221260737)
XLA Ops:
  0.6 145.2 %mixers.1 = (bf16[64,64]{1,0:T(8,128)(2,1)}, f32[2,2,256,128]{3,2,1,0:T(8,128)}, bf16[2,3,2,256]{3,2,1,0:T(2,128)(2,1)}, bf16[2,3,2,128]{3,2,1,0:T(2,128)(2,1)}, bf16[2,3,2,128]{3,2,1,0:T(2,128)(2,1)}) custom-call(bf16[64,64]{1,0:T(8,128)(2,1)} %hidden.1, s32[2]{0:T(128)} %lengths.1, f32[2,64]{1,0:T(2,128)} %in_gain.1, bf16[2,64,256]{2,1,0:T(8,128)(2,1)} %w_gate.1, ...), custom_call_target="tpu_custom_call" | custom-call | tf_op jit(solution)/shard_map/mixers/pallas_call | solution.py:390
  145.9 0.0 copy-start
  145.9 0.7 copy-done
  146.6 0.6 copy.31
  147.2 0.0 copy-start.1
  147.2 1.9 %copy.32 = f32[2,2,4,64,128]{4,3,2,1,0:T(8,128)} copy(f32[2,2,4,64,128]{4,3,2,1,0:T(8,128)} %bitcast.11) | data formatting | bytes 1048576
  149.1 0.0 copy-done.1
  149.1 0.0 copy-start.3
  149.1 0.6 copy.33
  149.7 0.1 copy-done.3
  149.8 0.0 copy-start.2
  149.8 0.6 copy.34
  150.4 0.1 copy-done.2
  150.4 0.6 copy.35
Async XLA Ops:
  145.9 0.7 copy-start
  147.2 1.9 %copy-start.1 = (bf16[2,3,2,256]{3,2,1,0:T(2,128)(2,1)S(1)}, bf16[2,3,2,256]{3,2,1,0:T(2,128)(2,1)}, u32[]{:S(2)}) copy-start(bf16[2,3,2,256]{3,2,1,0:T(2,128)(2,1)} %get-tuple-element.12) | copy-start | bytes 18436
  149.1 0.7 copy-start.3
  149.8 0.7 copy-start.2

commit v2 on v1

--- a/solution.py
+++ b/solution.py
@@ -37,9 +37,45 @@
     return jnp.concatenate([block[first : first + 1], block[first + 1 : first + 2]], axis=1)
 
 
-def kernel(
+def flush(*refs):
+    count = len(refs) // 2
+    sems = refs[-1]
+    copies = [pltpu.make_async_copy(refs[i], refs[count + i], sems.at[i]) for i in range(count)]
+    for c in copies:
+        c.start()
+    for c in copies:
+        c.wait()
+
+
+def kernel(n_dp, n_tp, *refs):
+    given, rest = refs[:21], refs[21:]
+    outs, held, rest = rest[:5], rest[5:24], rest[24:]
+    scratch, in_sem = rest[:-1], rest[-1]
+    lengths, state_in = given[1], given[17]
+    whole = [g for i, g in enumerate(given) if i not in (1, 17)]
+    barrier = pltpu.get_barrier_semaphore()
+    dp, tp = lax.axis_index("dp"), lax.axis_index("tp")
+    state = scratch[9]
+    loads = [pltpu.make_async_copy(g, h, in_sem.at[i]) for i, (g, h) in enumerate(zip(whole, held))]
+    loads.append(pltpu.make_async_copy(state_in, state, in_sem.at[len(whole)]))
+    for c in loads[:8]:
+        c.start()
+    for o in far_first(n_dp):
+        pl.semaphore_signal(barrier, inc=1, device_id={"dp": lax.rem(dp + o, n_dp)}, device_id_type=MESH)
+    for c in loads[8:]:
+        c.start()
+    for o in far_first(n_tp):
+        pl.semaphore_signal(barrier, inc=1, device_id={"tp": lax.rem(tp + o, n_tp)}, device_id_type=MESH)
+    held = list(held)
+    held.insert(1, lengths)
+    body(n_dp, n_tp, barrier, loads, *held, *outs, *scratch)
+
+
+def body(
     n_dp,
     n_tp,
+    barrier,
+    loads,
     hidden,
     lengths,
     in_gain,
@@ -57,12 +93,11 @@
     log_decay,
     group_gain,
     w_out,
-    state_in,
     hist_value,
     hist_write,
     hist_read,
     stream_out,
-    state_out,
+    state_new,
     buf_value,
     buf_write,
     buf_read,
@@ -74,14 +109,13 @@
     gathered,
     ar_send,
     ar_recv,
+    spare,
     state,
-    state_new,
     state_hi,
     state_lo,
     w_pack,
     conv_base,
     conv_last,
-    tap_rows,
     decay_pad,
     head_pad,
     rs_ssem,
@@ -90,8 +124,6 @@
     ag_rsem,
     ar_ssem,
     ar_rsem,
-    state_isem,
-    state_osem,
 ):
     dp, tp = lax.axis_index("dp"), lax.axis_index("tp")
     layers, feats = in_gain.shape
@@ -102,15 +134,6 @@
     head_dim = inner // heads
     depth = hist_value.shape[1]
     half = seqs // 2
-
-    barrier = pltpu.get_barrier_semaphore()
-    for o in far_first(n_dp):
-        pl.semaphore_signal(barrier, inc=1, device_id={"dp": lax.rem(dp + o, n_dp)}, device_id_type=MESH)
-    for o in far_first(n_tp):
-        pl.semaphore_signal(barrier, inc=1, device_id={"tp": lax.rem(tp + o, n_tp)}, device_id_type=MESH)
-    loads = [pltpu.make_async_copy(state_in.at[l], state.at[l], state_isem.at[l]) for l in range(layers)]
-    for c in loads:
-        c.start()
 
     lane_seq = lax.broadcasted_iota(jnp.int32, (seqs, LANES), 1)
     lane_inner = lax.broadcasted_iota(jnp.int32, (2, inner), 1)
@@ -181,9 +204,13 @@
             ).start()
         ar_recv[l, tp] = ar_send[l]
 
+    for c in loads[:7]:
+        c.wait()
     x_bf = hidden[...]
     project(0, x_bf.astype(F32))
 
+    for c in loads[7:]:
+        c.wait()
     position = [lengths[s] - 1 for s in range(2)]
     row8 = lax.broadcasted_iota(jnp.int32, (8, log_decay.shape[2]), 0)
     lane_pos = lax.broadcasted_iota(jnp.int32, (8, log_decay.shape[2]), 1)
@@ -226,7 +253,6 @@
                     conv_base[l, at : at + 1, :] = total[s : s + 1, c * LANES : (c + 1) * LANES]
                     conv_last[l, at : at + 1, :] = tap[depth : depth + 1, c * LANES : (c + 1) * LANES]
     for l in range(layers):
-        loads[l].wait()
         high = state[l].astype(BF16)
         state_hi[l] = high
         state_lo[l] = (state[l] - high.astype(F32)).astype(BF16)
@@ -236,7 +262,6 @@
     row16 = lax.broadcasted_iota(jnp.int32, (2 * BLOCKS, LANES), 0)
     is_gate = lax.rem(row16, BLOCKS) < 2
     row_of8 = lax.broadcasted_iota(jnp.int32, (8, LANES), 0)
-    stores = []
     x_pack = jnp.concatenate([x_bf[:half].astype(F32), x_bf[half:].astype(F32)], axis=1)
     for l in range(layers):
         send_partials(l)
@@ -292,8 +317,6 @@
                         decay[s : s + 1, h : h + 1] * state[l, s, at, :]
                         + cols[j * head_dim : (j + 1) * head_dim, s : s + 1] * write
                     )
-        stores.append(pltpu.make_async_copy(state_new.at[l], state_out.at[l], state_osem.at[l]))
-        stores[-1].start()
         for k in range(depth - 1):
             buf_value[l, k] = hist_value[l, k + 1]
             buf_write[l, k] = hist_write[l, k + 1]
@@ -325,7 +348,6 @@
         wait_bytes(rs_send.at[l, pl.ds(0, n_dp - 1)], rs_ssem.at[l])
         wait_bytes(ag_recv.at[l, pl.ds(0, n_dp - 1)], ag_ssem.at[l])
         wait_bytes(ar_recv.at[l, pl.ds(0, n_tp - 1)], ar_ssem.at[l])
-        stores[l].wait()
 
 
 def on_device(
@@ -380,25 +402,20 @@
         history_write_rows.transpose(0, 2, 1, 3),
         history_read_rows.transpose(0, 2, 1, 3),
     )
-    vmem, anywhere = pl.BlockSpec(memory_space=pltpu.VMEM), pl.BlockSpec(memory_space=pl.ANY)
-    in_specs = [vmem] * len(operands)
+    vmem, hbm = pl.BlockSpec(memory_space=pltpu.VMEM), pl.BlockSpec(memory_space=pltpu.HBM)
+    in_specs = [hbm] * len(operands)
     in_specs[1] = pl.BlockSpec(memory_space=pltpu.SMEM)
-    in_specs[17] = anywhere
-    taken = lambda a: jax.ShapeDtypeStruct(a.shape, a.dtype)
+    results = [operands[i] for i in (0, 17, 18, 19, 20)]
     positions = position_log_decay.shape[1]
     dma = pltpu.SemaphoreType.DMA
-    stream, states, values, writes, reads = pl.pallas_call(
+    whole = [o for i, o in enumerate(operands) if i not in (1, 17)]
+    finished = pl.pallas_call(
         functools.partial(kernel, n_dp, n_tp),
-        out_shape=(
-            taken(hidden),
-            taken(operands[17]),
-            taken(operands[18]),
-            taken(operands[19]),
-            taken(operands[20]),
-        ),
+        out_shape=[pltpu.VMEM(r.shape, r.dtype) for r in results],
         in_specs=in_specs,
-        out_specs=(vmem, anywhere, vmem, vmem, vmem),
-        scratch_shapes=[
+        out_specs=[vmem] * len(results),
+        scratch_shapes=[pltpu.VMEM(o.shape, o.dtype) for o in whole]
+        + [
             pltpu.VMEM((seqs * BLOCKS, LANES), F32),
             pltpu.VMEM((layers, n_dp, 2 * BLOCKS, LANES), BF16),
             pltpu.VMEM((layers, n_dp, 2 * BLOCKS, LANES), BF16),
@@ -407,21 +424,32 @@
             pltpu.VMEM((seqs, inner), F32),
             pltpu.VMEM((layers, seqs // 2, 2 * feats), BF16),
             pltpu.VMEM((layers, n_tp, seqs // 2, 2 * feats), BF16),
-            pltpu.VMEM(state_shape, F32),
+            pltpu.VMEM((8, LANES), F32),
             pltpu.VMEM(state_shape, F32),
             pltpu.VMEM(state_shape, BF16),
             pltpu.VMEM(state_shape, BF16),
             pltpu.VMEM((layers, 2 * feats, 2 * inner), BF16),
             pltpu.VMEM((layers, 2 * BLOCKS, LANES), F32),
             pltpu.VMEM((layers, 2 * BLOCKS, LANES), F32),
-            pltpu.VMEM((8, LANES), F32),
             pltpu.VMEM((layers, LANES, positions), F32),
             pltpu.VMEM((layers, 8, LANES), F32),
         ]
-        + [dma((layers,))] * 8,
-        compiler_params=pltpu.CompilerParams(collective_id=0, has_side_effects=True),
+        + [dma((layers,))] * 6
+        + [dma((len(whole) + 1,))],
+        compiler_params=pltpu.CompilerParams(
+            collective_id=0, has_side_effects=True
+        ),
         name="mixers",
     )(*operands)
+    stream, states, values, writes, reads = pl.pallas_call(
+        flush,
+        out_shape=[jax.ShapeDtypeStruct(r.shape, r.dtype) for r in results],
+        in_specs=[vmem] * len(results),
+        out_specs=[hbm] * len(results),
+        scratch_shapes=[dma((len(results),))],
+        compiler_params=pltpu.CompilerParams(vmem_limit_bytes=4 * 1024 * 1024),
+        name="flush",
+    )(*finished)
     return (
         stream,
         states.reshape(recurrent_head_state.shape),

time: 151 us -> 146 us (0.967)
  local copies, waits for them, and re-layouts: 5.13 us -> 0 us
    unnamed x13 -> x0, local copies, waits for them, and re-layouts: 5.13 us -> none
    pallas_call x1 -> x2, Pallas kernels: 145 us -> 145 us  [the longest x1 144 us: on_device(): pl.pallas_call(functools.partial(kernel, n_dp, n_tp), out_shape=[pltpu.VM...]
where the time goes in v2:
time: 146 us
  Pallas kernels  145 us (99%)
    pallas_call x1, Pallas kernels, on_device(): pl.pallas_call(functools.partial(kernel, n_dp, n_tp), out_shape=[pltpu.VM...  144 us

profile of v2, /device:TPU:6, one launch (start us, length us, event | category | flops | bytes accessed | tf_op | source)
XLA Modules:
  0.0 145.9 jit_solution(15124041492384033456)
XLA Ops:
  0.6 144.4 %mixers.1 = (bf16[64,64]{1,0:T(8,128)(2,1)S(1)}, f32[2,2,256,128]{3,2,1,0:T(8,128)S(1)}, bf16[2,3,2,256]{3,2,1,0:T(2,128)(2,1)S(1)}, bf16[2,3,2,128]{3,2,1,0:T(2,128)(2,1)S(1)}, bf16[2,3,2,128]{3,2,1,0:T(2,128)(2,1)S(1)}) custom-call(bf16[64,64]{1,0:T(8,128)(2,1)} %refs_0_.1, s32[2]{0:T(128)} %refs_1_.1, f32[2,64]{1,0:T(2,128)} %refs_2_.1, ...), custom_call_target="tpu_custom_call" | custom-call | tf_op jit(solution)/shard_map/mixers/pallas_call | solution.py:412
  145.1 0.9 flush.1

commit v3 on v2

--- a/solution.py
+++ b/solution.py
@@ -49,25 +49,23 @@
 
 def kernel(n_dp, n_tp, *refs):
     given, rest = refs[:21], refs[21:]
-    outs, held, rest = rest[:5], rest[5:24], rest[24:]
+    outs, held, rest = rest[:5], rest[5:25], rest[25:]
     scratch, in_sem = rest[:-1], rest[-1]
-    lengths, state_in = given[1], given[17]
-    whole = [g for i, g in enumerate(given) if i not in (1, 17)]
+    state_in = given[17]
+    whole = [g for i, g in enumerate(given) if i != 17]
     barrier = pltpu.get_barrier_semaphore()
     dp, tp = lax.axis_index("dp"), lax.axis_index("tp")
-    state = scratch[9]
+    state = scratch[15]
     loads = [pltpu.make_async_copy(g, h, in_sem.at[i]) for i, (g, h) in enumerate(zip(whole, held))]
     loads.append(pltpu.make_async_copy(state_in, state, in_sem.at[len(whole)]))
-    for c in loads[:8]:
+    for c in loads[:9]:
         c.start()
     for o in far_first(n_dp):
         pl.semaphore_signal(barrier, inc=1, device_id={"dp": lax.rem(dp + o, n_dp)}, device_id_type=MESH)
-    for c in loads[8:]:
+    for c in loads[9:]:
         c.start()
     for o in far_first(n_tp):
         pl.semaphore_signal(barrier, inc=1, device_id={"tp": lax.rem(tp + o, n_tp)}, device_id_type=MESH)
-    held = list(held)
-    held.insert(1, lengths)
     body(n_dp, n_tp, barrier, loads, *held, *outs, *scratch)
 
 
@@ -104,12 +102,18 @@
     part,
     rs_send,
     rs_recv,
+    rs_half_send,
+    rs_half_recv,
     ag_send,
+    ag_half_recv,
     ag_recv,
     gathered,
     ar_send,
     ar_recv,
-    spare,
+    w_pair,
+    w_pair_out,
+    x_mine,
+    x_other,
     state,
     state_hi,
     state_lo,
@@ -118,6 +122,16 @@
     conv_last,
     decay_pad,
     head_pad,
+    o_gate,
+    o_value,
+    o_write,
+    o_read,
+    o_step,
+    o_out,
+    o_gain,
+    o_hidden,
+    swap_ssem,
+    swap_rsem,
     rs_ssem,
     rs_rsem,
     ag_ssem,
@@ -135,7 +149,6 @@
     depth = hist_value.shape[1]
     half = seqs // 2
 
-    lane_seq = lax.broadcasted_iota(jnp.int32, (seqs, LANES), 1)
     lane_inner = lax.broadcasted_iota(jnp.int32, (2, inner), 1)
     pick = (
         lax.broadcasted_iota(jnp.int32, (w_step.shape[2], LANES), 0)
@@ -150,66 +163,58 @@
             out = jnp.where(lane < (h + 1) * head_dim, rows[:, h : h + 1], out)
         return out
 
-    def project(l, x):
-        normed = (x * in_gain[l : l + 1, :]).astype(BF16)
-        columns = []
-        for w in (w_gate, w_value, w_write, w_read):
-            r = jnp.dot(normed, w[l], preferred_element_type=F32)
-            for at in range(0, r.shape[1], LANES):
-                columns.append(r[:, at : at + LANES])
-        w_mine = jnp.dot(w_step[l], pick, preferred_element_type=F32).astype(BF16)
-        step = jnp.dot(normed, w_mine, preferred_element_type=F32)
-        square = jnp.sum(x * x, axis=1, keepdims=True)
-        rest = jnp.where(lane_seq == heads, square, step)
+    def lay_out(columns, count):
+        for c, column in enumerate(columns):
+            part[pl.ds(c, count, stride=BLOCKS), :] = column
+        return part[0 : count * BLOCKS, :].reshape(count // 2, 2 * BLOCKS, LANES).astype(BF16)
+
+    def with_rest(columns, step, square):
+        lane = lax.broadcasted_iota(jnp.int32, step.shape, 1)
+        rest = jnp.where(lane == heads, square, step)
         high = high_part(rest)
-        columns += [high, rest - high]
-        for c, column in enumerate(columns):
-            part[pl.ds(c, seqs, stride=BLOCKS), :] = column
-        rs_send[l] = part[...].reshape(n_dp, 2 * BLOCKS, LANES).astype(BF16)
-
-    def send_partials(l):
-        for o in far_first(n_dp):
-            to = lax.rem(dp + o, n_dp)
-            pltpu.make_async_remote_copy(
-                src_ref=rs_send.at[l, to],
-                dst_ref=rs_recv.at[l, dp],
-                send_sem=rs_ssem.at[l],
-                recv_sem=rs_rsem.at[l],
-                device_id={"dp": to},
-                device_id_type=MESH,
-            ).start()
-        rs_recv[l, dp] = rs_send[l, dp]
-
-    def send_gated(l):
-        for o in far_first(n_dp):
-            pltpu.make_async_remote_copy(
-                src_ref=ag_send.at[l],
-                dst_ref=ag_recv.at[l, dp],
-                send_sem=ag_ssem.at[l],
-                recv_sem=ag_rsem.at[l],
-                device_id={"dp": lax.rem(dp + o, n_dp)},
-                device_id_type=MESH,
-            ).start()
-        ag_recv[l, dp] = ag_send[l]
+        return columns + [high, rest - high]
+
+    def cut(r):
+        return [r[:, at : at + LANES] for at in range(0, r.shape[1], LANES)]
+
+    def send(src, dst, ssem, rsem, **to):
+        pltpu.make_async_remote_copy(
+            src_ref=src, dst_ref=dst, send_sem=ssem, recv_sem=rsem, device_id=to, device_id_type=MESH
+        ).start()
+
+    chip, core = dp // 2, lax.rem(dp, 2)
+    chips = n_dp // 2
+    sibling = dp + 1 - 2 * core
+    my_half, my_place = dp // chips, lax.rem(dp, chips)
+    served_here = my_half == core
+
+    def wait_half(ref, sem):
+        @pl.when(served_here)
+        def _():
+            wait_bytes(ref.at[pl.ds(0, chips - 1)], sem)
+
+        @pl.when(jnp.logical_not(served_here))
+        def _():
+            wait_bytes(ref, sem)
 
     def send_branch(l):
         for o in far_first(n_tp):
-            pltpu.make_async_remote_copy(
-                src_ref=ar_send.at[l],
-                dst_ref=ar_recv.at[l, tp],
-                send_sem=ar_ssem.at[l],
-                recv_sem=ar_rsem.at[l],
-                device_id={"tp": lax.rem(tp + o, n_tp)},
-                device_id_type=MESH,
-            ).start()
+            send(ar_send.at[l], ar_recv.at[l, tp], ar_ssem.at[l], ar_rsem.at[l], tp=lax.rem(tp + o, n_tp))
         ar_recv[l, tp] = ar_send[l]
 
-    for c in loads[:7]:
+    for c in loads[:8]:
         c.wait()
     x_bf = hidden[...]
-    project(0, x_bf.astype(F32))
-
-    for c in loads[7:]:
+    x = x_bf.astype(F32)
+    normed = (x * in_gain[0:1, :]).astype(BF16)
+    columns = []
+    for w in (w_gate, w_value, w_write, w_read):
+        columns += cut(jnp.dot(normed, w[0], preferred_element_type=F32))
+    w_mine = jnp.dot(w_step[0], pick, preferred_element_type=F32).astype(BF16)
+    step = jnp.dot(normed, w_mine, preferred_element_type=F32)
+    rs_send[...] = lay_out(with_rest(columns, step, jnp.sum(x * x, axis=1, keepdims=True)), seqs)
+
+    for c in loads[8:]:
         c.wait()
     position = [lengths[s] - 1 for s in range(2)]
     row8 = lax.broadcasted_iota(jnp.int32, (8, log_decay.shape[2]), 0)
@@ -222,6 +227,18 @@
     decay_pad[...] = jnp.zeros_like(decay_pad)
     head_pad[...] = jnp.zeros_like(head_pad)
     w_pack[...] = jnp.zeros_like(w_pack)
+    w_pack[0:feats, 0:inner] = w_out[1]
+    w_pack[feats : 2 * feats, inner : 2 * inner] = w_out[1]
+
+    def keep_pair(first, gate, value, write, read, step, out):
+        at, to = slice(first, first + feats), 0
+        mine = jnp.dot(step, pick, preferred_element_type=F32).astype(BF16)
+        for w in (gate, value, write, read, mine):
+            w_pair[at, to : to + w.shape[1]] = w
+            to += w.shape[1]
+        w_pair_out[at, :] = out
+
+    keep_pair(0, w_gate[1], w_value[1], w_write[1], w_read[1], w_step[1], w_out[0])
     decay_log = []
     for l in range(layers):
         decay_pad[l, 0:heads, :] = log_decay[l]
@@ -229,8 +246,6 @@
         decay_log.append(picked[0:2])
         head_pad[l, 0:1, 0:heads] = step_bias[l : l + 1, :]
         head_pad[l, 1:2, 0:heads] = jnp.exp(log_rate[l : l + 1, :])
-        w_pack[l, 0:feats, 0:inner] = w_out[l]
-        w_pack[l, feats : 2 * feats, inner : 2 * inner] = w_out[l]
         for taps, hist, row in (
             (taps_value, hist_value, 2),
             (taps_write, hist_write, 4),
@@ -262,11 +277,50 @@
     row16 = lax.broadcasted_iota(jnp.int32, (2 * BLOCKS, LANES), 0)
     is_gate = lax.rem(row16, BLOCKS) < 2
     row_of8 = lax.broadcasted_iota(jnp.int32, (8, LANES), 0)
-    x_pack = jnp.concatenate([x_bf[:half].astype(F32), x_bf[half:].astype(F32)], axis=1)
+    assert layers == 2
     for l in range(layers):
-        send_partials(l)
-        wait_bytes(rs_recv.at[l, pl.ds(0, n_dp - 1)], rs_rsem.at[l])
-        summed = jnp.sum(rs_recv[l].astype(F32), axis=0)
+        if l == 0:
+            for o in far_first(n_dp):
+                to = lax.rem(dp + o, n_dp)
+                send(rs_send.at[to], rs_recv.at[dp], rs_ssem.at[l], rs_rsem.at[l], dp=to)
+            rs_recv[dp] = rs_send[dp]
+            swaps = (
+                (w_gate.at[1], o_gate),
+                (w_value.at[1], o_value),
+                (w_write.at[1], o_write),
+                (w_read.at[1], o_read),
+                (w_step.at[1], o_step),
+                (w_out.at[0], o_out),
+                (in_gain, o_gain),
+                (hidden, o_hidden),
+            )
+            for i, (src, dst) in enumerate(swaps):
+                send(src, dst, swap_ssem.at[i], swap_rsem.at[i], dp=sibling)
+            wait_bytes(rs_recv.at[pl.ds(0, n_dp - 1)], rs_rsem.at[l])
+            received = rs_recv[...]
+        else:
+
+            @pl.when(jnp.logical_not(served_here))
+            def _():
+                send(
+                    rs_half_send.at[my_place],
+                    rs_half_recv.at[chip],
+                    rs_ssem.at[1],
+                    rs_rsem.at[1],
+                    dp=core * chips + my_place,
+                )
+
+            @pl.when(served_here)
+            def _():
+                rs_half_recv[chip] = rs_half_send[my_place]
+
+            for o in far_first(chips):
+                to = lax.rem(my_place + o, chips)
+                send(rs_half_send.at[to], rs_half_recv.at[chip], rs_ssem.at[l], rs_rsem.at[l], dp=core * chips + to)
+            send(x_mine, x_other, swap_ssem.at[8], swap_rsem.at[8], dp=sibling)
+            wait_half(rs_half_recv, rs_rsem.at[l])
+            received = rs_half_recv[...]
+        summed = jnp.sum(received.astype(F32), axis=0)
         rest = jnp.concatenate(
             [summed[BLOCKS * s + 6 : BLOCKS * s + 7] + summed[BLOCKS * s + 7 : BLOCKS * s + 8] for s in range(2)], axis=0
         )
@@ -300,7 +354,22 @@
         mean = jnp.sum(mixed * mixed, axis=1, keepdims=True) / inner
         gated = mixed * lax.rsqrt(mean + epsilon) * group_gain[l : l + 1, :]
         ag_send[l] = gated.astype(BF16)
-        send_gated(l)
+        if l == 0:
+            for o in far_first(chips):
+                to = 2 * lax.rem(chip + o, chips) + my_half
+                send(ag_send.at[l], ag_half_recv.at[my_place], ag_ssem.at[l], ag_rsem.at[l], dp=to)
+
+            @pl.when(jnp.logical_not(served_here))
+            def _():
+                send(ag_send.at[0], ag_half_recv.at[my_place], ag_ssem.at[0], ag_rsem.at[0], dp=sibling)
+
+            @pl.when(served_here)
+            def _():
+                ag_half_recv[my_place] = ag_send[0]
+        else:
+            for o in far_first(n_dp):
+                send(ag_send.at[l], ag_recv.at[dp], ag_ssem.at[l], ag_rsem.at[l], dp=lax.rem(dp + o, n_dp))
+            ag_recv[dp] = ag_send[l]
 
         for b in range(inner // LANES):
             cols = jnp.transpose(
@@ -331,23 +400,47 @@
             [current[BLOCKS * s + 5 : BLOCKS * s + 6] for s in range(2)], axis=0
         ).astype(BF16)
 
-        wait_bytes(ag_recv.at[l, pl.ds(0, n_dp - 1)], ag_rsem.at[l])
-        for d in range(n_dp):
-            gathered[2 * d : 2 * d + 2, :] = ag_recv[l, d].astype(F32)
-        rows = jnp.concatenate([gathered[0:half, :], gathered[half:, :]], axis=1).astype(BF16)
-        branch = lax.dot_general(rows, w_pack[l], LAST, preferred_element_type=F32)
-        ar_send[l] = branch.astype(BF16)
+        half_rows = pl.ds(pl.multiple_of(core * half, half), half)
+        if l == 0:
+            for i, (src, dst) in enumerate(swaps):
+                pltpu.make_async_copy(dst, dst, swap_rsem.at[i]).wait()
+            keep_pair(feats, o_gate[...], o_value[...], o_write[...], o_read[...], o_step[...], o_out[...])
+            pair_gain = jnp.concatenate([in_gain[1:2, :], o_gain[1:2, :]], axis=1)
+            x = jnp.concatenate([hidden[half_rows, :].astype(F32), o_hidden[half_rows, :].astype(F32)], axis=1)
+            wait_half(ag_half_recv, ag_rsem.at[l])
+            for d in range(chips):
+                gathered[2 * d : 2 * d + 2, :] = ag_half_recv[d].astype(F32)
+            rows, weight = gathered[0:half, :].astype(BF16), w_pair_out[...]
+        else:
+            wait_bytes(x_other, swap_rsem.at[8])
+            mine, other = x[:, :feats], x_other[...].astype(F32)[:, feats:]
+            is_first = core == 0
+            x = jnp.concatenate([jnp.where(is_first, mine, other), jnp.where(is_first, other, mine)], axis=1)
+            wait_bytes(ag_recv.at[pl.ds(0, n_dp - 1)], ag_rsem.at[l])
+            for d in range(n_dp):
+                gathered[2 * d : 2 * d + 2, :] = ag_recv[d].astype(F32)
+            rows = jnp.concatenate([gathered[0:half, :], gathered[half:, :]], axis=1).astype(BF16)
+            weight = w_pack[...]
+        ar_send[l] = lax.dot_general(rows, weight, LAST, preferred_element_type=F32).astype(BF16)
         send_branch(l)
         wait_bytes(ar_recv.at[l, pl.ds(0, n_tp - 1)], ar_rsem.at[l])
-        x_pack = high_part(x_pack + jnp.sum(ar_recv[l].astype(F32), axis=0))
-        x = jnp.concatenate([x_pack[:, :feats], x_pack[:, feats:]], axis=0)
-        if l + 1 < layers:
-            project(l + 1, x)
-    stream_out[...] = x.astype(BF16)
+        x = high_part(x + jnp.sum(ar_recv[l].astype(F32), axis=0))
+        if l == 0:
+            normed = (x * pair_gain).astype(BF16)
+            columns = cut(jnp.dot(normed, w_pair[...], preferred_element_type=F32))
+            step = columns.pop()
+            rs_half_send[...] = lay_out(with_rest(columns, step, jnp.sum(x * x, axis=1, keepdims=True)), half)
+            x_mine[...] = x.astype(BF16)
+    stream_out[...] = jnp.concatenate([x[:, :feats], x[:, feats:]], axis=0).astype(BF16)
+    wait_bytes(rs_send.at[pl.ds(0, n_dp - 1)], rs_ssem.at[0])
+    wait_half(rs_half_send, rs_ssem.at[1])
+    wait_half(ag_half_recv, ag_ssem.at[0])
+    wait_bytes(ag_recv.at[pl.ds(0, n_dp - 1)], ag_ssem.at[1])
     for l in range(layers):
-        wait_bytes(rs_send.at[l, pl.ds(0, n_dp - 1)], rs_ssem.at[l])
-        wait_bytes(ag_recv.at[l, pl.ds(0, n_dp - 1)], ag_ssem.at[l])
         wait_bytes(ar_recv.at[l, pl.ds(0, n_tp - 1)], ar_ssem.at[l])
+    for i, (src, dst) in enumerate(swaps):
+        pltpu.make_async_copy(src, src, swap_ssem.at[i]).wait()
+    wait_bytes(x_mine, swap_ssem.at[8])
 
 
 def on_device(
@@ -404,35 +497,49 @@
     )
     vmem, hbm = pl.BlockSpec(memory_space=pltpu.VMEM), pl.BlockSpec(memory_space=pltpu.HBM)
     in_specs = [hbm] * len(operands)
-    in_specs[1] = pl.BlockSpec(memory_space=pltpu.SMEM)
     results = [operands[i] for i in (0, 17, 18, 19, 20)]
     positions = position_log_decay.shape[1]
     dma = pltpu.SemaphoreType.DMA
-    whole = [o for i, o in enumerate(operands) if i not in (1, 17)]
+    whole = [o for i, o in enumerate(operands) if i != 17]
+    space = lambda o: pltpu.SMEM if o is lengths else pltpu.VMEM
     finished = pl.pallas_call(
         functools.partial(kernel, n_dp, n_tp),
         out_shape=[pltpu.VMEM(r.shape, r.dtype) for r in results],
         in_specs=in_specs,
         out_specs=[vmem] * len(results),
-        scratch_shapes=[pltpu.VMEM(o.shape, o.dtype) for o in whole]
+        scratch_shapes=[space(o)(o.shape, o.dtype) for o in whole]
         + [
             pltpu.VMEM((seqs * BLOCKS, LANES), F32),
-            pltpu.VMEM((layers, n_dp, 2 * BLOCKS, LANES), BF16),
-            pltpu.VMEM((layers, n_dp, 2 * BLOCKS, LANES), BF16),
+            pltpu.VMEM((n_dp, 2 * BLOCKS, LANES), BF16),
+            pltpu.VMEM((n_dp, 2 * BLOCKS, LANES), BF16),
+            pltpu.VMEM((n_dp // 2, 2 * BLOCKS, LANES), BF16),
+            pltpu.VMEM((n_dp // 2, 2 * BLOCKS, LANES), BF16),
             pltpu.VMEM((layers, 2, inner), BF16),
-            pltpu.VMEM((layers, n_dp, 2, inner), BF16),
+            pltpu.VMEM((n_dp // 2, 2, inner), BF16),
+            pltpu.VMEM((n_dp, 2, inner), BF16),
             pltpu.VMEM((seqs, inner), F32),
             pltpu.VMEM((layers, seqs // 2, 2 * feats), BF16),
             pltpu.VMEM((layers, n_tp, seqs // 2, 2 * feats), BF16),
-            pltpu.VMEM((8, LANES), F32),
+            pltpu.VMEM((2 * feats, 7 * LANES), BF16),
+            pltpu.VMEM((2 * feats, inner), BF16),
+            pltpu.VMEM((seqs // 2, 2 * feats), BF16),
+            pltpu.VMEM((seqs // 2, 2 * feats), BF16),
             pltpu.VMEM(state_shape, F32),
             pltpu.VMEM(state_shape, BF16),
             pltpu.VMEM(state_shape, BF16),
-            pltpu.VMEM((layers, 2 * feats, 2 * inner), BF16),
+            pltpu.VMEM((2 * feats, 2 * inner), BF16),
             pltpu.VMEM((layers, 2 * BLOCKS, LANES), F32),
             pltpu.VMEM((layers, 2 * BLOCKS, LANES), F32),
             pltpu.VMEM((layers, LANES, positions), F32),
             pltpu.VMEM((layers, 8, LANES), F32),
+        ]
+        + [pltpu.VMEM(o.shape[1:], o.dtype) for o in (gate_matrix, input_matrix, write_matrix, read_matrix, step_matrix)]
+        + [
+            pltpu.VMEM(operands[16].shape[1:], BF16),
+            pltpu.VMEM(input_norm_gain.shape, F32),
+            pltpu.VMEM(hidden.shape, BF16),
+            dma((9,)),
+            dma((9,)),
         ]
         + [dma((layers,))] * 6
         + [dma((len(whole) + 1,))],

time: 146 us -> 143 us (0.979)
  Pallas kernels: 145 us -> 142 us
    pallas_call x1, Pallas kernels: 144 us -> 141 us  [on_device(): pl.pallas_call(functools.partial(kernel, n_dp, n_tp), out_shape=[pltpu.VM...]
where the time goes in v3:
time: 143 us
  Pallas kernels  142 us (99%)
    pallas_call x1, Pallas kernels, on_device(): pl.pallas_call(functools.partial(kernel, n_dp, n_tp), out_shape=[pltpu.VM...  141 us

profile of v3, /device:TPU:6, one launch (start us, length us, event | category | flops | bytes accessed | tf_op | source)
XLA Modules:
  0.0 142.9 jit_solution(4424119801842978972)
XLA Ops:
  0.6 141.4 %mixers.1 = (bf16[64,64]{1,0:T(8,128)(2,1)S(1)}, f32[2,2,256,128]{3,2,1,0:T(8,128)S(1)}, bf16[2,3,2,256]{3,2,1,0:T(2,128)(2,1)S(1)}, bf16[2,3,2,128]{3,2,1,0:T(2,128)(2,1)S(1)}, bf16[2,3,2,128]{3,2,1,0:T(2,128)(2,1)S(1)}) custom-call(bf16[64,64]{1,0:T(8,128)(2,1)} %refs_0_.1, s32[2]{0:T(128)} %refs_1_.1, f32[2,64]{1,0:T(2,128)} %refs_2_.1, ...), custom_call_target="tpu_custom_call" | custom-call | tf_op jit(solution)/shard_map/mixers/pallas_call | solution.py:505
  142.0 0.9 flush.1

commit v4 on v3

--- a/solution.py
+++ b/solution.py
@@ -64,8 +64,12 @@
         pl.semaphore_signal(barrier, inc=1, device_id={"dp": lax.rem(dp + o, n_dp)}, device_id_type=MESH)
     for c in loads[9:]:
         c.start()
-    for o in far_first(n_tp):
-        pl.semaphore_signal(barrier, inc=1, device_id={"tp": lax.rem(tp + o, n_tp)}, device_id_type=MESH)
+    for z in range(n_tp - 1, 0, -1):
+
+        @pl.when(z > tp)
+        def _(z=z):
+            pl.semaphore_signal(barrier, inc=1, device_id={"tp": z}, device_id_type=MESH)
+
     body(n_dp, n_tp, barrier, loads, *held, *outs, *scratch)
 
 
@@ -138,6 +142,7 @@
     ag_rsem,
     ar_ssem,
     ar_rsem,
+    entered,
 ):
     dp, tp = lax.axis_index("dp"), lax.axis_index("tp")
     layers, feats = in_gain.shape
@@ -272,7 +277,7 @@
         state_hi[l] = high
         state_lo[l] = (state[l] - high.astype(F32)).astype(BF16)
 
-    pl.semaphore_wait(barrier, n_dp - 1 + n_tp - 1)
+    pl.semaphore_wait(barrier, n_dp - 1 + tp)
 
     row16 = lax.broadcasted_iota(jnp.int32, (2 * BLOCKS, LANES), 0)
     is_gate = lax.rem(row16, BLOCKS) < 2
@@ -284,6 +289,12 @@
                 to = lax.rem(dp + o, n_dp)
                 send(rs_send.at[to], rs_recv.at[dp], rs_ssem.at[l], rs_rsem.at[l], dp=to)
             rs_recv[dp] = rs_send[dp]
+            for z in range(n_tp - 1):
+
+                @pl.when(z < tp)
+                def _(z=z):
+                    pl.semaphore_signal(entered, inc=1, device_id={"tp": z}, device_id_type=MESH)
+
             swaps = (
                 (w_gate.at[1], o_gate),
                 (w_value.at[1], o_value),
@@ -422,6 +433,12 @@
             rows = jnp.concatenate([gathered[0:half, :], gathered[half:, :]], axis=1).astype(BF16)
             weight = w_pack[...]
         ar_send[l] = lax.dot_general(rows, weight, LAST, preferred_element_type=F32).astype(BF16)
+        if l == 0:
+
+            @pl.when(tp < n_tp - 1)
+            def _():
+                pl.semaphore_wait(entered, n_tp - 1 - tp)
+
         send_branch(l)
         wait_bytes(ar_recv.at[l, pl.ds(0, n_tp - 1)], ar_rsem.at[l])
         x = high_part(x + jnp.sum(ar_recv[l].astype(F32), axis=0))
@@ -542,6 +559,7 @@
             dma((9,)),
         ]
         + [dma((layers,))] * 6
+        + [pltpu.SemaphoreType.REGULAR]
         + [dma((len(whole) + 1,))],
         compiler_params=pltpu.CompilerParams(
             collective_id=0, has_side_effects=True

time: 143 us -> 141 us (0.986)
  Pallas kernels: 142 us -> 140 us
    pallas_call x1, Pallas kernels: 141 us -> 139 us  [on_device(): pl.pallas_call(functools.partial(kernel, n_dp, n_tp), out_shape=[pltpu.VM...]
where the time goes in v4:
time: 141 us
  Pallas kernels  140 us (99%)
    pallas_call x1, Pallas kernels, on_device(): pl.pallas_call(functools.partial(kernel, n_dp, n_tp), out_shape=[pltpu.VM...  139 us

profile of v4, /device:TPU:6, one launch (start us, length us, event | category | flops | bytes accessed | tf_op | source)
XLA Modules:
  0.0 140.7 jit_solution(13727092856874665866)
XLA Ops:
  0.6 139.2 %mixers.1 = (bf16[64,64]{1,0:T(8,128)(2,1)S(1)}, f32[2,2,256,128]{3,2,1,0:T(8,128)S(1)}, bf16[2,3,2,256]{3,2,1,0:T(2,128)(2,1)S(1)}, bf16[2,3,2,128]{3,2,1,0:T(2,128)(2,1)S(1)}, bf16[2,3,2,128]{3,2,1,0:T(2,128)(2,1)S(1)}) custom-call(bf16[64,64]{1,0:T(8,128)(2,1)} %refs_0_.1, s32[2]{0:T(128)} %refs_1_.1, f32[2,64]{1,0:T(2,128)} %refs_2_.1, ...), custom_call_target="tpu_custom_call" | custom-call | tf_op jit(solution)/shard_map/mixers/pallas_call | solution.py:522
  139.8 0.9 flush.1

commit v5 on v4

--- a/solution.py
+++ b/solution.py
@@ -55,7 +55,7 @@
     whole = [g for i, g in enumerate(given) if i != 17]
     barrier = pltpu.get_barrier_semaphore()
     dp, tp = lax.axis_index("dp"), lax.axis_index("tp")
-    state = scratch[15]
+    state = scratch[17]
     loads = [pltpu.make_async_copy(g, h, in_sem.at[i]) for i, (g, h) in enumerate(zip(whole, held))]
     loads.append(pltpu.make_async_copy(state_in, state, in_sem.at[len(whole)]))
     for c in loads[:9]:
@@ -118,6 +118,8 @@
     w_pair_out,
     x_mine,
     x_other,
+    x_last,
+    x_given,
     state,
     state_hi,
     state_lo,
@@ -143,6 +145,8 @@
     ar_ssem,
     ar_rsem,
     entered,
+    last_ssem,
+    last_rsem,
 ):
     dp, tp = lax.axis_index("dp"), lax.axis_index("tp")
     layers, feats = in_gain.shape
@@ -202,10 +206,6 @@
         def _():
             wait_bytes(ref, sem)
 
-    def send_branch(l):
-        for o in far_first(n_tp):
-            send(ar_send.at[l], ar_recv.at[l, tp], ar_ssem.at[l], ar_rsem.at[l], tp=lax.rem(tp + o, n_tp))
-        ar_recv[l, tp] = ar_send[l]
 
     for c in loads[:8]:
         c.wait()
@@ -378,8 +378,12 @@
             def _():
                 ag_half_recv[my_place] = ag_send[0]
         else:
-            for o in far_first(n_dp):
-                send(ag_send.at[l], ag_recv.at[dp], ag_ssem.at[l], ag_rsem.at[l], dp=lax.rem(dp + o, n_dp))
+            for d in range(n_dp):
+
+                @pl.when(dp != d)
+                def _(d=d):
+                    send(ag_send.at[1], ag_recv.at[dp], ag_ssem.at[1], ag_rsem.at[1], dp=d)
+
             ag_recv[dp] = ag_send[l]
 
         for b in range(inner // LANES):
@@ -439,25 +443,70 @@
             def _():
                 pl.semaphore_wait(entered, n_tp - 1 - tp)
 
-        send_branch(l)
-        wait_bytes(ar_recv.at[l, pl.ds(0, n_tp - 1)], ar_rsem.at[l])
-        x = high_part(x + jnp.sum(ar_recv[l].astype(F32), axis=0))
-        if l == 0:
+            for o in far_first(n_tp):
+                send(ar_send.at[l], ar_recv.at[l, tp], ar_ssem.at[l], ar_rsem.at[l], tp=lax.rem(tp + o, n_tp))
+            ar_recv[l, tp] = ar_send[l]
+            wait_bytes(ar_recv.at[l, pl.ds(0, n_tp - 1)], ar_rsem.at[l])
+            x = high_part(x + jnp.sum(ar_recv[l].astype(F32), axis=0))
             normed = (x * pair_gain).astype(BF16)
             columns = cut(jnp.dot(normed, w_pair[...], preferred_element_type=F32))
             step = columns.pop()
             rs_half_send[...] = lay_out(with_rest(columns, step, jnp.sum(x * x, axis=1, keepdims=True)), half)
             x_mine[...] = x.astype(BF16)
-    stream_out[...] = jnp.concatenate([x[:, :feats], x[:, feats:]], axis=0).astype(BF16)
+
+    giver = min(2, n_tp - 1)
+    is_first_row, is_giver = tp == 0, tp == giver
+    is_taker = jnp.logical_not(jnp.logical_or(is_first_row, is_giver))
+
+    def put_out(rows):
+        stream_out[...] = jnp.concatenate([rows[:, :feats], rows[:, feats:]], axis=0).astype(BF16)
+
+    def summed_stream():
+        wait_bytes(ar_recv.at[1, pl.ds(0, n_tp - 1)], ar_rsem.at[1])
+        return high_part(x + jnp.sum(ar_recv[1].astype(F32), axis=0))
+
+    for z in (0, giver):
+
+        @pl.when(tp != z)
+        def _(z=z):
+            send(ar_send.at[1], ar_recv.at[1, tp], ar_ssem.at[1], ar_rsem.at[1], tp=z)
+
+    ar_recv[1, tp] = ar_send[1]
     wait_bytes(rs_send.at[pl.ds(0, n_dp - 1)], rs_ssem.at[0])
     wait_half(rs_half_send, rs_ssem.at[1])
     wait_half(ag_half_recv, ag_ssem.at[0])
     wait_bytes(ag_recv.at[pl.ds(0, n_dp - 1)], ag_ssem.at[1])
-    for l in range(layers):
-        wait_bytes(ar_recv.at[l, pl.ds(0, n_tp - 1)], ar_ssem.at[l])
+    wait_bytes(ar_recv.at[0, pl.ds(0, n_tp - 1)], ar_ssem.at[0])
     for i, (src, dst) in enumerate(swaps):
         pltpu.make_async_copy(src, src, swap_ssem.at[i]).wait()
     wait_bytes(x_mine, swap_ssem.at[8])
+
+    @pl.when(is_taker)
+    def _():
+        wait_bytes(ar_recv.at[0, pl.ds(0, 2)], ar_ssem.at[1])
+
+    @pl.when(jnp.logical_not(is_taker))
+    def _():
+        wait_bytes(ar_send.at[1], ar_ssem.at[1])
+
+    @pl.when(is_first_row)
+    def _():
+        put_out(summed_stream())
+
+    @pl.when(is_giver)
+    def _():
+        last = summed_stream()
+        x_last[...] = last.astype(BF16)
+        for z in range(1, n_tp):
+            if z != giver:
+                send(x_last, x_given, last_ssem, last_rsem, tp=z)
+        put_out(last)
+        wait_bytes(ar_recv.at[1, pl.ds(0, n_tp - 2)], last_ssem)
+
+    @pl.when(is_taker)
+    def _():
+        wait_bytes(x_given, last_rsem)
+        put_out(x_given[...].astype(F32))
 
 
 def on_device(
@@ -541,6 +590,8 @@
             pltpu.VMEM((2 * feats, inner), BF16),
             pltpu.VMEM((seqs // 2, 2 * feats), BF16),
             pltpu.VMEM((seqs // 2, 2 * feats), BF16),
+            pltpu.VMEM((seqs // 2, 2 * feats), BF16),
+            pltpu.VMEM((seqs // 2, 2 * feats), BF16),
             pltpu.VMEM(state_shape, F32),
             pltpu.VMEM(state_shape, BF16),
             pltpu.VMEM(state_shape, BF16),
@@ -559,7 +610,7 @@
             dma((9,)),
         ]
         + [dma((layers,))] * 6
-        + [pltpu.SemaphoreType.REGULAR]
+        + [pltpu.SemaphoreType.REGULAR, dma, dma]
         + [dma((len(whole) + 1,))],
         compiler_params=pltpu.CompilerParams(
             collective_id=0, has_side_effects=True

time: 141 us -> 139 us (0.986)
  Pallas kernels: 140 us -> 138 us
    pallas_call x1, Pallas kernels: 139 us -> 137 us  [on_device(): pl.pallas_call(functools.partial(kernel, n_dp, n_tp), out_shape=[pltpu.VM...]
where the time goes in v5:
time: 139 us
  Pallas kernels  138 us (99%)
    pallas_call x1, Pallas kernels, on_device(): pl.pallas_call(functools.partial(kernel, n_dp, n_tp), out_shape=[pltpu.VM...  137 us

profile of v5, /device:TPU:6, one launch (start us, length us, event | category | flops | bytes accessed | tf_op | source)
XLA Modules:
  0.0 138.5 jit_solution(9052346966760702160)
XLA Ops:
  0.6 137.0 %mixers.1 = (bf16[64,64]{1,0:T(8,128)(2,1)S(1)}, f32[2,2,256,128]{3,2,1,0:T(8,128)S(1)}, bf16[2,3,2,256]{3,2,1,0:T(2,128)(2,1)S(1)}, bf16[2,3,2,128]{3,2,1,0:T(2,128)(2,1)S(1)}, bf16[2,3,2,128]{3,2,1,0:T(2,128)(2,1)S(1)}) custom-call(bf16[64,64]{1,0:T(8,128)(2,1)} %refs_0_.1, s32[2]{0:T(128)} %refs_1_.1, f32[2,64]{1,0:T(2,128)} %refs_2_.1, ...), custom_call_target="tpu_custom_call" | custom-call | tf_op jit(solution)/shard_map/mixers/pallas_call | solution.py:571
  137.7 0.9 flush.1

commit v6 on v5

--- a/solution.py
+++ b/solution.py
@@ -305,29 +305,24 @@
                 (in_gain, o_gain),
                 (hidden, o_hidden),
             )
-            for i, (src, dst) in enumerate(swaps):
-                send(src, dst, swap_ssem.at[i], swap_rsem.at[i], dp=sibling)
             wait_bytes(rs_recv.at[pl.ds(0, n_dp - 1)], rs_rsem.at[l])
             received = rs_recv[...]
         else:
 
+            crossed = lax.rem(my_half + core, 2) * (chips // 2)
+            for o in far_first(chips):
+                to = lax.rem(my_place + o + crossed, chips)
+                send(rs_half_send.at[to], rs_half_recv.at[chip], rs_ssem.at[l], rs_rsem.at[l], dp=core * chips + to)
+
             @pl.when(jnp.logical_not(served_here))
             def _():
-                send(
-                    rs_half_send.at[my_place],
-                    rs_half_recv.at[chip],
-                    rs_ssem.at[1],
-                    rs_rsem.at[1],
-                    dp=core * chips + my_place,
-                )
+                to = lax.rem(my_place + chips // 2, chips)
+                send(rs_half_send.at[to], rs_half_recv.at[chip], rs_ssem.at[1], rs_rsem.at[1], dp=core * chips + to)
 
             @pl.when(served_here)
             def _():
                 rs_half_recv[chip] = rs_half_send[my_place]
 
-            for o in far_first(chips):
-                to = lax.rem(my_place + o, chips)
-                send(rs_half_send.at[to], rs_half_recv.at[chip], rs_ssem.at[l], rs_rsem.at[l], dp=core * chips + to)
             send(x_mine, x_other, swap_ssem.at[8], swap_rsem.at[8], dp=sibling)
             wait_half(rs_half_recv, rs_rsem.at[l])
             received = rs_half_recv[...]
@@ -377,6 +372,9 @@
             @pl.when(served_here)
             def _():
                 ag_half_recv[my_place] = ag_send[0]
+
+            for i, (src, dst) in enumerate(swaps):
+                send(src, dst, swap_ssem.at[i], swap_rsem.at[i], dp=sibling)
         else:
             for d in range(n_dp):
 

time: 139 us -> 139 us (level)
  no operation moved by 1% of the time
where the time goes in v6:
time: 139 us; the launch traced here: 138 us
  Pallas kernels  138 us (99%)
    pallas_call x1, Pallas kernels, on_device(): pl.pallas_call(functools.partial(kernel, n_dp, n_tp), out_shape=[pltpu.VM...  137 us

profile of v6, /device:TPU:6, one launch (start us, length us, event | category | flops | bytes accessed | tf_op | source)
XLA Modules:
  0.0 138.2 jit_solution(13569892217540380552)
XLA Ops:
  0.6 136.7 %mixers.1 = (bf16[64,64]{1,0:T(8,128)(2,1)S(1)}, f32[2,2,256,128]{3,2,1,0:T(8,128)S(1)}, bf16[2,3,2,256]{3,2,1,0:T(2,128)(2,1)S(1)}, bf16[2,3,2,128]{3,2,1,0:T(2,128)(2,1)S(1)}, bf16[2,3,2,128]{3,2,1,0:T(2,128)(2,1)S(1)}) custom-call(bf16[64,64]{1,0:T(8,128)(2,1)} %refs_0_.1, s32[2]{0:T(128)} %refs_1_.1, f32[2,64]{1,0:T(2,128)} %refs_2_.1, ...), custom_call_target="tpu_custom_call" | custom-call | tf_op jit(solution)/shard_map/mixers/pallas_call | solution.py:569
  137.3 0.9 flush.1
